TPU v7x, 32 devices: a whole 2x2x4 slice. The times are simulated.
32 devices in a mesh: grp: 2 (over x), ep: 8 (over z, y), tp: 2 (over core).
Axes of the slice: x: 2, y: 2, z: 4, core: 2. Of those that a mesh axis runs over, the one named last changes fastest.
Arguments:
- hidden_in: bfloat16 [256, 2048], P(('grp', 'ep', 'tp')), parts along dimension 0, may hold values from -6 to 6
- query_nope: bfloat16 [256, 16, 64], P(('grp', 'ep', 'tp')), parts along dimension 0, may hold values from -102 to 102
- query_rope: bfloat16 [256, 16, 32], P(('grp', 'ep', 'tp')), parts along dimension 0, may hold values from -6 to 6
- new_latent: bfloat16 [256, 256], P(('grp', 'ep', 'tp')), parts along dimension 0, may hold values from -6 to 6
- new_rope: bfloat16 [256, 32], P(('grp', 'ep', 'tp')), parts along dimension 0, may hold values from -6 to 6
- cache_latent: bfloat16 [256, 1024, 256], P(('grp', 'ep', 'tp')), parts along dimension 0, may hold values from -6 to 6
- cache_rope: bfloat16 [256, 1024, 32], P(('grp', 'ep', 'tp')), parts along dimension 0, may hold values from -6 to 6
- lengths: int32 [256], P(('grp', 'ep', 'tp')), parts along dimension 0, may hold values from 1 to 1024, as said below
- absorb_key: bfloat16 [256, 16, 64], replicated, may hold values from -0.75 to 0.75
- value_up: bfloat16 [256, 16, 128], replicated, may hold values from -0.375 to 0.375
- out_proj: bfloat16 [2048, 2048], P(None, ('ep', 'tp')), may hold values from -0.125 to 0.125
- gain_mix: bfloat16 [2048], replicated, may hold values from 0.099609375 to 1.8984375
- gain_ffn_in: bfloat16 [2048], replicated, may hold values from 0.099609375 to 1.8984375
- router: bfloat16 [2048, 16], replicated, may hold values from -0.125 to 0.125
- routes: int32 [256, 6], P(('grp', 'ep')), parts along dimension 0, may hold values from 0 to 15, all different within a row; in each aligned block of 16 rows (0 to 15, 16 to 31, ...) at most 12 rows name the same one
- expert_gate: bfloat16 [16, 2048, 256], P(('ep', 'tp')), may hold values from -0.125 to 0.125
- expert_up: bfloat16 [16, 2048, 256], P(('ep', 'tp')), may hold values from -0.125 to 0.125
- expert_down: bfloat16 [16, 256, 2048], P(('ep', 'tp')), may hold values from -0.375 to 0.375
- shared_gate: bfloat16 [2048, 256], replicated, may hold values from -0.125 to 0.125
- shared_up: bfloat16 [2048, 256], replicated, may hold values from -0.125 to 0.125
- shared_down: bfloat16 [256, 2048], replicated, may hold values from -0.375 to 0.375
- gain_ffn_out: bfloat16 [2048], replicated, may hold values from 0.099609375 to 1.8984375
Outputs:
- layer_out: bfloat16 [256, 2048], P(('grp', 'ep', 'tp')), parts along dimension 0
There are 2 independent parts, one for each index of `grp`. A program takes and returns all parts, laid end to end along the dimension named above; an argument that names none is the same for every part. Nothing has to cross between parts.
Inputs may be any that keep to these rules, and one draw needn't show every extreme that they name: `lengths`: every sequence holds 1 to 1024 cached positions, and some sequence holds 1024. `routes`: each row names 6 different experts; in each aligned block of 16 rows (the rows of one index of ep) no expert is named by more than 12 rows, and in some block some expert is named by exactly 12 rows.
All inputs are finite; a program needn't handle non-finite values.
Results may differ from a plain program's by a relative error of at most 0.015.
Values may be sent and summed in bfloat16 or wider, within the bound.
A program may use at most 64 MiB of HBM per device.

v0:
```python
import functools

import jax
import jax.numpy as jnp
from jax import lax
from jax.experimental import pallas as pl
from jax.experimental.pallas import tpu as pltpu
from jax.sharding import PartitionSpec as P

ABLK = 512


rope_theta = 10000.0
norm_eps = 1e-06
routed_scale = 2.5
masked_score = -1e30


def normalize(values):
    return values * lax.rsqrt(jnp.mean(values * values, axis=-1, keepdims=True) + norm_eps)


def rotate(values, positions):
    half_dim = values.shape[-1] // 2
    inverse = rope_theta ** (-jnp.arange(half_dim, dtype=jnp.float32) * 2.0 / values.shape[-1])
    angles = positions * inverse
    cosine = jnp.cos(angles)
    sine_table = jnp.sin(angles)
    first_half = values[..., :half_dim]
    second_half = values[..., half_dim:]
    return jnp.concatenate(
        [
            first_half * cosine - second_half * sine_table,
            first_half * sine_table + second_half * cosine,
        ],
        axis=-1,
    )


def swiglu(flat_rows, gate_w, up_w, down_w):
    gate_part = jnp.dot(flat_rows, gate_w, preferred_element_type=jnp.float32)
    up_part = jnp.dot(flat_rows, up_w, preferred_element_type=jnp.float32)
    inner_rows = (jax.nn.silu(gate_part) * up_part).astype(jnp.bfloat16)
    return jnp.dot(inner_rows, down_w, preferred_element_type=jnp.float32).astype(jnp.bfloat16)


def local_wide(
    hidden_in,
    query_nope,
    query_rope,
    new_latent,
    new_rope,
    cache_latent,
    cache_rope,
    lengths,
    absorb_key,
    value_up,
    out_proj,
    gain_mix,
    gain_ffn_in,
    router,
    routes,
    expert_gate,
    expert_up,
    expert_down,
    shared_gate,
    shared_up,
    shared_down,
    gain_ffn_out,
):
    seq_count = hidden_in.shape[0]
    positions = lengths.astype(jnp.float32)
    query_latent = jnp.einsum(
        "shn,chn->shc", query_nope, absorb_key, preferred_element_type=jnp.float32
    ).astype(jnp.bfloat16)
    query_pe = rotate(query_rope.astype(jnp.float32), positions[:, None, None]).astype(jnp.bfloat16)
    latent_new = normalize(new_latent.astype(jnp.float32)).astype(jnp.bfloat16)
    key_new = rotate(new_rope.astype(jnp.float32), positions[:, None]).astype(jnp.bfloat16)
    score_scale = (query_nope.shape[-1] + query_rope.shape[-1]) ** (-0.5)
    new_score = (
        jnp.einsum("shc,sc->sh", query_latent, latent_new, preferred_element_type=jnp.float32)
        + jnp.einsum("shr,sr->sh", query_pe, key_new, preferred_element_type=jnp.float32)
    ) * score_scale

    def attend_block(block_index, loop_state):
        running_max, weight_total, weighted_sum = loop_state
        block_start = block_index * ABLK
        block_latent = lax.dynamic_slice_in_dim(cache_latent, block_start, ABLK, 1)
        block_rope = lax.dynamic_slice_in_dim(cache_rope, block_start, ABLK, 1)
        scores = (
            jnp.einsum(
                "shc,skc->shk", query_latent, block_latent, preferred_element_type=jnp.float32
            )
            + jnp.einsum("shr,skr->shk", query_pe, block_rope, preferred_element_type=jnp.float32)
        ) * score_scale
        key_index = block_start + lax.iota(jnp.int32, ABLK)
        in_range = key_index[None, None, :] < lengths[:, None, None]
        scores = jnp.where(in_range, scores, masked_score)
        new_max = jnp.maximum(running_max, jnp.max(scores, axis=-1))
        rescale = jnp.exp(running_max - new_max)
        weights = jnp.exp(scores - new_max[..., None])
        weight_total = weight_total * rescale + jnp.sum(weights, axis=-1)
        weighted_sum = weighted_sum * rescale[..., None] + jnp.einsum(
            "shk,skc->shc",
            weights.astype(jnp.bfloat16),
            block_latent,
            preferred_element_type=jnp.float32,
        )
        return (new_max, weight_total, weighted_sum)

    longest = jnp.max(lengths)
    block_count = (longest + ABLK - 1) // ABLK
    ones_start = jnp.ones_like(new_score)
    sum_start = ones_start[..., None] * latent_new.astype(jnp.float32)[:, None, :]
    final_max, weight_total, weighted_sum = lax.fori_loop(
        0, block_count, attend_block, (new_score, ones_start, sum_start)
    )
    latent_out = (weighted_sum / weight_total[..., None]).astype(jnp.bfloat16)
    heads_out = (
        jnp.einsum("shc,chv->shv", latent_out, value_up, preferred_element_type=jnp.float32)
        .astype(jnp.bfloat16)
        .reshape(seq_count, -1)
    )
    column_rows = jnp.dot(
        lax.all_gather(heads_out, ("ep", "tp"), axis=0, tiled=True),
        out_proj,
        preferred_element_type=jnp.float32,
    ).astype(jnp.bfloat16)
    mixed_rows = lax.all_to_all(column_rows, ("ep", "tp"), split_axis=0, concat_axis=1, tiled=True)
    after_mix = (
        hidden_in.astype(jnp.float32)
        + gain_mix.astype(jnp.float32) * normalize(mixed_rows.astype(jnp.float32))
    ).astype(jnp.bfloat16)
    ffn_in = (normalize(after_mix.astype(jnp.float32)) * gain_ffn_in.astype(jnp.float32)).astype(
        jnp.bfloat16
    )
    affinity = jax.nn.sigmoid(jnp.dot(ffn_in, router, preferred_element_type=jnp.float32))
    experts_total = router.shape[1]
    own_start = lax.axis_index("tp") * seq_count
    own_routes = lax.dynamic_slice_in_dim(routes, own_start, seq_count, 0)
    choose = own_routes[..., None] == lax.iota(jnp.int32, experts_total)[None, None, :]
    chosen = jnp.sum(jnp.where(choose, affinity[:, None, :], 0.0), axis=-1)
    route_weights = chosen / jnp.sum(chosen, axis=-1, keepdims=True) * routed_scale
    group_rows, top_count = routes.shape
    capacity = 2 * ((group_rows * top_count + experts_total - 1) // experts_total)
    flat_routes = routes.reshape(-1)
    order_index = lax.iota(jnp.int32, group_rows * top_count)
    same_expert = flat_routes[:, None] == flat_routes[None, :]
    earlier = order_index[None, :] < order_index[:, None]
    slot_number = jnp.sum(jnp.logical_and(same_expert, earlier), axis=1)
    slot_number = slot_number.reshape(group_rows, top_count)
    own_slots = lax.dynamic_slice_in_dim(slot_number, own_start, seq_count, 0)
    slot_index = own_routes * capacity + own_slots
    slots_total = experts_total * capacity
    slot_table = jnp.any(
        slot_index[None, :, :] == lax.iota(jnp.int32, slots_total)[:, None, None], axis=-1
    ).astype(jnp.bfloat16)
    outgoing_terms = jnp.dot(slot_table, ffn_in, preferred_element_type=jnp.float32)
    outgoing = outgoing_terms.astype(jnp.bfloat16).reshape(experts_total, capacity, -1)
    received = lax.all_to_all(outgoing, ("ep", "tp"), split_axis=0, concat_axis=0, tiled=True)
    ep_count = lax.axis_size("ep")
    tp_count = lax.axis_size("tp")
    item_count = received.shape[1]
    width = received.shape[2]
    merged = jnp.sum(received.reshape(ep_count, tp_count, item_count, width), axis=1)
    outputs = swiglu(
        merged.reshape(ep_count * item_count, width), expert_gate[0], expert_up[0], expert_down[0]
    )
    copies = jnp.broadcast_to(
        outputs.reshape(ep_count, 1, item_count, width), (ep_count, tp_count, item_count, width)
    )
    copies = copies.reshape(ep_count * tp_count, item_count, width)
    returned = lax.all_to_all(copies, ("ep", "tp"), split_axis=0, concat_axis=0, tiled=True)
    picked = returned.reshape(slots_total, -1)[slot_index]
    routed = jnp.sum(picked.astype(jnp.float32) * route_weights[..., None], axis=1)
    shared = swiglu(ffn_in, shared_gate, shared_up, shared_down)
    combined = routed + shared.astype(jnp.float32)
    return (
        after_mix.astype(jnp.float32) + gain_ffn_out.astype(jnp.float32) * normalize(combined)
    ).astype(jnp.bfloat16)


def fused_kernel(
    grid_p,
    grid_q,
    score_scale,
    hidden_ref,
    qn_ref,
    qr_ref,
    nl_ref,
    nr_ref,
    len_ref,
    routes_ref,
    gm_ref,
    gf_ref,
    go_ref,
    ab_hbm,
    cl_hbm,
    cr_hbm,
    vup_hbm,
    wo_hbm,
    router_hbm,
    eg_hbm,
    eu_hbm,
    ed_hbm,
    sg_hbm,
    su_hbm,
    sd_hbm,
    out_ref,
    cl,
    cr,
    vup,
    wide_up,
    ql_ref,
    qp_ref,
    ab,
    vraw,
    wo,
    router,
    eg,
    eu,
    ed,
    sg,
    su,
    sd,
    xbuf,
    hbuf,
    cbuf,
    lat,
    norm_rows,
    mix_rows,
    terms,
    sib,
    part,
    back,
    cache_sem,
    rope_sem,
    weight_sem,
    ag_send,
    ag_recv,
    sib_send,
    sib_recv,
    back_send,
    back_recv,
):
    seq_count, heads, nope = qn_ref.shape
    rope = qr_ref.shape[2]
    width = out_ref.shape[1]
    ep_count = grid_p * grid_q
    device_count = 2 * ep_count
    total_rows = device_count * seq_count
    me_e = lax.axis_index("ep")
    me_t = lax.axis_index("tp")
    other_t = 1 - me_t
    p = me_e // grid_q
    q = me_e % grid_q
    me = me_e * 2 + me_t

    def device(e, t):
        return {"ep": e, "tp": t}

    sibling = device(me_e, other_t)
    barrier = pltpu.get_barrier_semaphore()
    for step in range(1, ep_count):
        pl.semaphore_signal(
            barrier,
            inc=1,
            device_id=device((me_e + step) % ep_count, me_t),
            device_id_type=pl.DeviceIdType.MESH,
        )
    pl.semaphore_signal(
        barrier, inc=1, device_id=sibling, device_id_type=pl.DeviceIdType.MESH
    )

    early_copies = []
    for index, (source, target) in enumerate(((ab_hbm, ab), (vup_hbm, vraw))):
        copy = pltpu.make_async_copy(source, target, weight_sem.at[index])
        copy.start()
        early_copies.append(copy)
    cache_copies = []
    for s in range(seq_count):
        pair = (
            pltpu.make_async_copy(cl_hbm.at[s], cl.at[s], cache_sem.at[s]),
            pltpu.make_async_copy(cr_hbm.at[s], cr.at[s], rope_sem.at[s]),
        )
        pair[0].start()
        pair[1].start()
        cache_copies.append(pair)
    weight_copies = []
    moves = (
        (wo_hbm, wo),
        (router_hbm, router),
        (eg_hbm, eg),
        (eu_hbm, eu),
        (ed_hbm, ed),
        (sg_hbm, sg),
        (su_hbm, su),
        (sd_hbm, sd),
    )
    for index, (source, target) in enumerate(moves):
        copy = pltpu.make_async_copy(source, target, weight_sem.at[index + 2])
        copy.start()
        weight_copies.append(copy)

    xbuf[me, :, 0:width] = hidden_ref[...]
    mark_shape = (seq_count, xbuf.shape[2] - width)
    mark_row = lax.broadcasted_iota(jnp.int32, mark_shape, 0)
    mark_lane = lax.broadcasted_iota(jnp.int32, mark_shape, 1)
    marks = jnp.zeros(mark_shape, jnp.float32)
    for s in range(seq_count):
        for j in range(routes_ref.shape[0]):
            expert = routes_ref[j, me_t * seq_count + s]
            marks = jnp.where((mark_row == s) & (mark_lane == expert), 1.0, marks)
    xbuf[me, :, width:] = marks.astype(jnp.bfloat16)

    line_steps = list(range(1, grid_p))
    pending = []

    class Gather:
        def __init__(self, buf, which):
            self.buf, self.which, self.count = buf, which, 0

        def send(self, slot, target):
            copy = pltpu.make_async_remote_copy(
                src_ref=self.buf.at[slot],
                dst_ref=self.buf.at[slot],
                send_sem=ag_send.at[self.which, self.count],
                recv_sem=ag_recv.at[self.which, slot],
                device_id=target,
                device_id_type=pl.DeviceIdType.MESH,
            )
            copy.start()
            pending.append(copy)
            self.count += 1

        def arrive(self, slot):
            pltpu.make_async_remote_copy(
                src_ref=self.buf.at[slot],
                dst_ref=self.buf.at[slot],
                send_sem=ag_send.at[self.which, 0],
                recv_sem=ag_recv.at[self.which, slot],
                device_id=sibling,
                device_id_type=pl.DeviceIdType.MESH,
            ).wait_recv()

        def line(self, step):
            return (p + step) % grid_p

        def first(self):
            for step in sorted(line_steps, key=lambda v: -min(v, grid_p - v)):
                self.send(me, device(self.line(step) * grid_q + q, me_t))
            for turn in range(1, grid_q):
                self.send(me, device(p * grid_q + (q + turn) % grid_q, me_t))
            self.send(me, sibling)

        def second(self):
            for step in sorted(line_steps, key=lambda v: min(v, grid_p - v)):
                slot = (self.line(step) * grid_q + q) * 2 + me_t
                self.arrive(slot)
                for turn in range(1, grid_q):
                    self.send(slot, device(p * grid_q + (q + turn) % grid_q, me_t))
                self.send(slot, sibling)

        def third(self):
            for step in sorted([0] + line_steps, key=lambda v: min(v, grid_p - v)):
                for turn in range(1, grid_q):
                    slot = (self.line(step) * grid_q + (q + turn) % grid_q) * 2 + me_t
                    self.arrive(slot)
                    self.send(slot, sibling)

        def last(self):
            for e in range(ep_count):
                self.arrive(e * 2 + other_t)

    rows_gather = Gather(xbuf, 0)
    pl.semaphore_wait(barrier, ep_count)
    rows_gather.first()

    half = rope // 2
    turn_row = lax.broadcasted_iota(jnp.int32, (seq_count, rope), 0)
    turn_lane = lax.broadcasted_iota(jnp.int32, (seq_count, rope), 1)
    position = jnp.zeros((seq_count, rope), jnp.float32)
    for s in range(seq_count):
        position = jnp.where(turn_row == s, len_ref[s].astype(jnp.float32), position)
    inverse = jnp.zeros((seq_count, rope), jnp.float32)
    for i in range(half):
        inverse = jnp.where(turn_lane % half == i, rope_theta ** (-2.0 * i / rope), inverse)
    angles = position * inverse
    cosine = jnp.cos(angles)
    sine = jnp.sin(angles) * jnp.where(turn_lane < half, -1.0, 1.0)

    def turned(values, cos_rows, sin_rows):
        swapped = jnp.concatenate([values[:, half:], values[:, :half]], axis=1)
        return values * cos_rows + swapped * sin_rows

    def per_head(table):
        return jnp.broadcast_to(table[:, None, :], (seq_count, heads, rope)).reshape(
            seq_count * heads, rope
        )

    query_rows = qr_ref[...].astype(jnp.float32).reshape(seq_count * heads, rope)
    qp_ref[...] = turned(query_rows, per_head(cosine), per_head(sine)).astype(jnp.bfloat16)
    key_rows = turned(nr_ref[...].astype(jnp.float32), cosine, sine).astype(jnp.bfloat16)
    key_rows = key_rows.astype(jnp.float32)
    new_rows = normalize(nl_ref[...].astype(jnp.float32)).astype(jnp.bfloat16).astype(jnp.float32)

    nope_rows = qn_ref[...].astype(jnp.float32).reshape(seq_count * heads, nope)
    row_head = lax.broadcasted_iota(jnp.int32, (seq_count * heads, 2 * nope), 0) % heads
    pair_lane = lax.broadcasted_iota(jnp.int32, (seq_count * heads, 2 * nope), 1) // nope
    doubled = jnp.concatenate([nope_rows, nope_rows], axis=1)
    spread_query = jnp.concatenate(
        [
            jnp.where(row_head == pair_lane + 2 * j, doubled, 0.0).astype(jnp.bfloat16)
            for j in range(heads // 2)
        ],
        axis=1,
    )
    early_copies[0].wait()
    ql_ref[...] = jnp.dot(spread_query, ab[...], preferred_element_type=jnp.float32).astype(
        jnp.bfloat16
    )

    context = cl.shape[1]
    key_index = lax.broadcasted_iota(jnp.int32, (heads, context), 1)

    def attend(s):
        cache_copies[s][0].wait()
        cache_copies[s][1].wait()
        q_lat = ql_ref[s * heads : (s + 1) * heads, :]
        q_pe = qp_ref[s * heads : (s + 1) * heads, :]
        keys = cl[s]
        dims = (((1,), (1,)), ((), ()))
        scores = (
            lax.dot_general(q_lat, keys, dims, preferred_element_type=jnp.float32)
            + jnp.dot(q_pe, cr[s], preferred_element_type=jnp.float32)
        ) * score_scale
        new_row = new_rows[s : s + 1, :]
        key_row = key_rows[s : s + 1, :]
        new_score = (
            jnp.sum(q_lat.astype(jnp.float32) * new_row, axis=-1, keepdims=True)
            + jnp.sum(q_pe.astype(jnp.float32) * key_row, axis=-1, keepdims=True)
        ) * score_scale
        scores = jnp.where(key_index < len_ref[s], scores, masked_score)
        row_max = jnp.maximum(jnp.max(scores, axis=-1, keepdims=True), new_score)
        weights = jnp.exp(scores - row_max)
        new_weight = jnp.exp(new_score - row_max)
        weight_total = jnp.sum(weights, axis=-1, keepdims=True) + new_weight
        weighted = jnp.dot(weights.astype(jnp.bfloat16), keys, preferred_element_type=jnp.float32)
        weighted = weighted + new_weight.astype(jnp.bfloat16).astype(jnp.float32) * new_row
        lat[s * heads : (s + 1) * heads, :] = (weighted / weight_total).astype(jnp.bfloat16)

    early_copies[1].wait()
    value_dim = vraw.shape[2]
    wide_up[...] = vraw[...].astype(jnp.float32)
    for h in range(heads):
        vup[:, h * value_dim : (h + 1) * value_dim] = wide_up[:, h, :].astype(jnp.bfloat16)
    cut_a = seq_count // 2
    for s in range(cut_a):
        attend(s)
    rows_gather.second()
    for s in range(cut_a, seq_count):
        attend(s)

    spread = jnp.dot(lat[...], vup[...], preferred_element_type=jnp.float32)
    own_heads = []
    head_row = lax.broadcasted_iota(jnp.int32, (seq_count, heads, value_dim), 1)
    for h in range(heads):
        block = spread[:, h * value_dim : (h + 1) * value_dim].reshape(seq_count, heads, value_dim)
        own_heads.append(jnp.sum(jnp.where(head_row == h, block, 0.0), axis=1))
    hbuf[me] = jnp.concatenate(own_heads, axis=1).astype(jnp.bfloat16)
    heads_gather = Gather(hbuf, 1)
    heads_gather.first()
    rows_gather.third()
    heads_gather.second()
    heads_gather.third()
    rows_gather.last()
    weight_copies[0].wait()
    heads_gather.last()

    flat_heads = hbuf[...].reshape(total_rows, hbuf.shape[2])
    cbuf[me] = jnp.dot(flat_heads, wo[...], preferred_element_type=jnp.float32).astype(jnp.bfloat16)
    columns_gather = Gather(cbuf, 2)
    columns_gather.first()
    columns_gather.second()
    columns_gather.third()
    columns_gather.last()

    gains = [
        ref[...].astype(jnp.float32).reshape(1, width) for ref in (gm_ref, gf_ref, go_ref)
    ]
    mixed = jnp.concatenate([cbuf[o] for o in range(device_count)], axis=1).astype(jnp.float32)
    stage = xbuf[...].reshape(total_rows, xbuf.shape[2])
    after_mix = (stage[:, :width].astype(jnp.float32) + gains[0] * normalize(mixed)).astype(
        jnp.bfloat16
    )
    mix_rows[...] = after_mix.reshape(mix_rows.shape)
    ffn_in = (normalize(after_mix.astype(jnp.float32)) * gains[1]).astype(jnp.bfloat16)
    norm_rows[...] = ffn_in.reshape(norm_rows.shape)
    weight_copies[1].wait()
    affinity = jax.nn.sigmoid(
        lax.dot_general(
            ffn_in, router[...], (((1,), (1,)), ((), ())), preferred_element_type=jnp.float32
        )
    )
    hot = stage[:, width : width + affinity.shape[1]].astype(jnp.float32)
    chosen = affinity * hot
    lane = lax.broadcasted_iota(jnp.int32, chosen.shape, 1)
    mine = jnp.sum(jnp.where(lane == me, chosen, 0.0), axis=1, keepdims=True)
    mine = mine / jnp.sum(chosen, axis=1, keepdims=True) * routed_scale
    for copy in weight_copies[2:5]:
        copy.wait()
    expert_out = swiglu(ffn_in, eg[...], eu[...], ed[...])
    scaled = (expert_out.astype(jnp.float32) * mine).astype(jnp.bfloat16)
    terms[...] = scaled.reshape(terms.shape)

    def to_sibling(step):
        e = (me_e + step) % ep_count
        return pltpu.make_async_remote_copy(
            src_ref=terms.at[e * 2 + other_t],
            dst_ref=sib.at[e],
            send_sem=sib_send.at[step],
            recv_sem=sib_recv.at[e],
            device_id=sibling,
            device_id_type=pl.DeviceIdType.MESH,
        )

    order = sorted(range(1, ep_count), key=lambda v: -min(v, ep_count - v)) + [0]
    sib_copies = [to_sibling(step) for step in order]
    for copy in sib_copies:
        copy.start()
    sends = []
    for step in order:
        e = (me_e + step) % ep_count
        to_sibling(step).wait_recv()
        paired = terms[e * 2 + me_t].astype(jnp.float32) + sib[e].astype(jnp.float32)
        if step == 0:
            routed = paired
        else:
            part[e] = paired.astype(jnp.bfloat16)
            copy = pltpu.make_async_remote_copy(
                src_ref=part.at[e],
                dst_ref=back.at[me_e],
                send_sem=back_send.at[step],
                recv_sem=back_recv.at[me_e],
                device_id=device(e, me_t),
                device_id_type=pl.DeviceIdType.MESH,
            )
            copy.start()
            sends.append(copy)
    for copy in weight_copies[5:8]:
        copy.wait()
    combined = routed + swiglu(norm_rows[me], sg[...], su[...], sd[...]).astype(jnp.float32)
    for step in reversed(order[:-1]):
        e = (me_e + step) % ep_count
        pltpu.make_async_remote_copy(
            src_ref=part.at[e],
            dst_ref=back.at[e],
            send_sem=back_send.at[step],
            recv_sem=back_recv.at[e],
            device_id=device(e, me_t),
            device_id_type=pl.DeviceIdType.MESH,
        ).wait_recv()
        combined = combined + back[e].astype(jnp.float32)
    out_ref[...] = (
        mix_rows[me].astype(jnp.float32) + gains[2] * normalize(combined)
    ).astype(jnp.bfloat16)
    for copy in pending + sib_copies + sends:
        copy.wait_send()


def local_fused(
    hidden_in,
    query_nope,
    query_rope,
    new_latent,
    new_rope,
    cache_latent,
    cache_rope,
    lengths,
    absorb_key,
    value_up,
    out_proj,
    gain_mix,
    gain_ffn_in,
    router,
    routes,
    expert_gate,
    expert_up,
    expert_down,
    shared_gate,
    shared_up,
    shared_down,
    gain_ffn_out,
):
    seq_count, width = hidden_in.shape
    heads, latent = query_nope.shape[1], cache_latent.shape[2]
    ep_count = lax.axis_size("ep")
    device_count = 2 * ep_count
    bits = (ep_count - 1).bit_length()
    grid_p = 2 ** ((bits + 1) // 2)
    grid_q = ep_count // grid_p
    bf = jnp.bfloat16
    score_scale = (query_nope.shape[-1] + query_rope.shape[-1]) ** (-0.5)
    sends = (grid_p - 1) + grid_p * (grid_q - 1) + ep_count
    big = pl.BlockSpec(memory_space=pl.ANY)
    near = pl.BlockSpec(memory_space=pltpu.VMEM)
    dma = pltpu.SemaphoreType.DMA
    total_rows = device_count * seq_count
    rope_rows = jnp.swapaxes(cache_rope, 1, 2)
    router_rows = jnp.swapaxes(router, 0, 1)
    absorb_rows = jnp.transpose(absorb_key, (1, 2, 0)).reshape(-1, latent)
    own_shape = (seq_count, width + 128)
    weights = (
        out_proj,
        router_rows,
        expert_gate[0],
        expert_up[0],
        expert_down[0],
        shared_gate,
        shared_up,
        shared_down,
    )
    operands = (
        hidden_in,
        query_nope,
        query_rope,
        new_latent,
        new_rope,
        lengths,
        jnp.swapaxes(routes, 0, 1),
        gain_mix,
        gain_ffn_in,
        gain_ffn_out,
        absorb_rows,
        cache_latent,
        rope_rows,
        value_up,
    ) + weights
    scalar = pl.BlockSpec(memory_space=pltpu.SMEM)
    specs = [near] * 5 + [scalar] * 2 + [near] * 3 + [big] * 12
    flops = 2 * total_rows * width * out_proj.shape[1]
    return pl.pallas_call(
        functools.partial(fused_kernel, grid_p, grid_q, score_scale),
        out_shape=jax.ShapeDtypeStruct((seq_count, width), bf),
        in_specs=specs,
        out_specs=near,
        scratch_shapes=[
            pltpu.VMEM(cache_latent.shape, bf),
            pltpu.VMEM(rope_rows.shape, bf),
            pltpu.VMEM((latent, value_up.shape[1] * value_up.shape[2]), bf),
            pltpu.VMEM(value_up.shape, jnp.float32),
            pltpu.VMEM((seq_count * heads, latent), bf),
            pltpu.VMEM((seq_count * heads, query_rope.shape[2]), bf),
            pltpu.VMEM(absorb_rows.shape, bf),
            pltpu.VMEM(value_up.shape, bf),
        ]
        + [pltpu.VMEM(w.shape, bf) for w in weights]
        + [
            pltpu.VMEM((device_count,) + own_shape, bf),
            pltpu.VMEM((device_count, seq_count, out_proj.shape[0]), bf),
            pltpu.VMEM((device_count, total_rows, out_proj.shape[1]), bf),
            pltpu.VMEM((seq_count * heads, latent), bf),
            pltpu.VMEM((device_count, seq_count, width), bf),
            pltpu.VMEM((device_count, seq_count, width), bf),
            pltpu.VMEM((device_count, seq_count, width), bf),
            pltpu.VMEM((ep_count, seq_count, width), bf),
            pltpu.VMEM((ep_count, seq_count, width), bf),
            pltpu.VMEM((ep_count, seq_count, width), bf),
            dma((seq_count,)),
            dma((seq_count,)),
            dma((len(weights) + 2,)),
            dma((3, sends)),
            dma((3, device_count)),
            dma((ep_count,)),
            dma((ep_count,)),
            dma((ep_count,)),
            dma((ep_count,)),
        ],
        compiler_params=pltpu.CompilerParams(
            collective_id=0, has_side_effects=True, vmem_limit_bytes=56 * 2**20
        ),
        cost_estimate=pl.CostEstimate(flops=flops, bytes_accessed=2**24, transcendentals=0),
        name="layer_step",
    )(*operands)


def local(*args):
    hidden_in, out_proj, router = args[0], args[10], args[13]
    device_count = lax.axis_size("ep") * lax.axis_size("tp")
    fits = (
        lax.axis_size("tp") == 2
        and hidden_in.shape[0] == 8
        and device_count * hidden_in.shape[0] <= 256
        and out_proj.shape[1] % 128 == 0
        and router.shape[1] == device_count
    )
    return local_fused(*args) if fits else local_wide(*args)


def solution(mesh):
    placed = (
        P(("grp", "ep", "tp"), None),
        P(("grp", "ep", "tp"), None, None),
        P(("grp", "ep", "tp"), None, None),
        P(("grp", "ep", "tp"), None),
        P(("grp", "ep", "tp"), None),
        P(("grp", "ep", "tp"), None, None),
        P(("grp", "ep", "tp"), None, None),
        P(("grp", "ep", "tp")),
        P(),
        P(),
        P(None, ("ep", "tp")),
        P(),
        P(),
        P(),
        P(("grp", "ep"), None),
        P(("ep", "tp"), None, None),
        P(("ep", "tp"), None, None),
        P(("ep", "tp"), None, None),
        P(),
        P(),
        P(),
        P(),
    )
    return jax.shard_map(
        local, mesh=mesh, in_specs=placed, out_specs=P(("grp", "ep", "tp"), None), check_vma=False
    )
```

profile of v0, /device:TPU:0, one launch (start us, length us, event | category | flops | bytes accessed | tf_op | source)
XLA Modules:
  0.0 47.0 jit_solution(5468926311698768754)
XLA Ops:
  0.0 45.6 %layer_step.1 = bf16[8,2048]{1,0:T(8,128)(2,1)} custom-call(bf16[8,2048]{1,0:T(8,128)(2,1)} %hidden_ref.1, bf16[8,16,64]{2,1,0:T(8,128)(2,1)} %qn_ref.1, bf16[8,16,32]{2,1,0:T(8,128)(2,1)} %qr_ref.1, bf16[8,256]{1,0:T(8,128)(2,1)} %nl_ref.1, bf16[8,32]{1,0:T(8,128)(2,1)} %nr_ref.1, s32[8]{0:T(128)} %len_ref.1, s32[6,16]{1,0:T(8,128)} %bitcast.15, ...), custom_call_target="tpu_custom_call" | custom-call | flops 67108864 | bytes 16777216 | tf_op jit(solution)/shard_map/layer_step/pallas_call | solution.py:642
  45.6 1.4 %copy.24 = bf16[8,2048]{1,0:T(8,128)(2,1)} copy(bf16[8,2048]{1,0:T(8,128)(2,1)} %layer_step.1) | data formatting | bytes 65536
where the time goes:
time: 47.2 us; the launch traced here: 47 us
  Pallas kernels  45.6 us (97%)
  local copies, waits for them, and re-layouts  1.38 us (3%)
    pallas_call x1, Pallas kernels, local_fused(): pl.pallas_call(functools.partial(fused_kernel, grid_p, grid_q, score_scal...  45.6 us
    unnamed x1, local copies, waits for them, and re-layouts  1.38 us

commit v1 on v0

v1 whole, which is shorter than its diff:
```python
import functools

import jax
import jax.numpy as jnp
from jax import lax
from jax.experimental import pallas as pl
from jax.experimental.pallas import tpu as pltpu
from jax.sharding import PartitionSpec as P

ABLK = 512


rope_theta = 10000.0
norm_eps = 1e-06
routed_scale = 2.5
masked_score = -1e30


def normalize(values):
    return values * lax.rsqrt(jnp.mean(values * values, axis=-1, keepdims=True) + norm_eps)


def rotate(values, positions):
    half_dim = values.shape[-1] // 2
    inverse = rope_theta ** (-jnp.arange(half_dim, dtype=jnp.float32) * 2.0 / values.shape[-1])
    angles = positions * inverse
    cosine = jnp.cos(angles)
    sine_table = jnp.sin(angles)
    first_half = values[..., :half_dim]
    second_half = values[..., half_dim:]
    return jnp.concatenate(
        [
            first_half * cosine - second_half * sine_table,
            first_half * sine_table + second_half * cosine,
        ],
        axis=-1,
    )


def swiglu(flat_rows, gate_w, up_w, down_w):
    gate_part = jnp.dot(flat_rows, gate_w, preferred_element_type=jnp.float32)
    up_part = jnp.dot(flat_rows, up_w, preferred_element_type=jnp.float32)
    inner_rows = (jax.nn.silu(gate_part) * up_part).astype(jnp.bfloat16)
    return jnp.dot(inner_rows, down_w, preferred_element_type=jnp.float32).astype(jnp.bfloat16)


def local_wide(
    hidden_in,
    query_nope,
    query_rope,
    new_latent,
    new_rope,
    cache_latent,
    cache_rope,
    lengths,
    absorb_key,
    value_up,
    out_proj,
    gain_mix,
    gain_ffn_in,
    router,
    routes,
    expert_gate,
    expert_up,
    expert_down,
    shared_gate,
    shared_up,
    shared_down,
    gain_ffn_out,
):
    seq_count = hidden_in.shape[0]
    positions = lengths.astype(jnp.float32)
    query_latent = jnp.einsum(
        "shn,chn->shc", query_nope, absorb_key, preferred_element_type=jnp.float32
    ).astype(jnp.bfloat16)
    query_pe = rotate(query_rope.astype(jnp.float32), positions[:, None, None]).astype(jnp.bfloat16)
    latent_new = normalize(new_latent.astype(jnp.float32)).astype(jnp.bfloat16)
    key_new = rotate(new_rope.astype(jnp.float32), positions[:, None]).astype(jnp.bfloat16)
    score_scale = (query_nope.shape[-1] + query_rope.shape[-1]) ** (-0.5)
    new_score = (
        jnp.einsum("shc,sc->sh", query_latent, latent_new, preferred_element_type=jnp.float32)
        + jnp.einsum("shr,sr->sh", query_pe, key_new, preferred_element_type=jnp.float32)
    ) * score_scale

    def attend_block(block_index, loop_state):
        running_max, weight_total, weighted_sum = loop_state
        block_start = block_index * ABLK
        block_latent = lax.dynamic_slice_in_dim(cache_latent, block_start, ABLK, 1)
        block_rope = lax.dynamic_slice_in_dim(cache_rope, block_start, ABLK, 1)
        scores = (
            jnp.einsum(
                "shc,skc->shk", query_latent, block_latent, preferred_element_type=jnp.float32
            )
            + jnp.einsum("shr,skr->shk", query_pe, block_rope, preferred_element_type=jnp.float32)
        ) * score_scale
        key_index = block_start + lax.iota(jnp.int32, ABLK)
        in_range = key_index[None, None, :] < lengths[:, None, None]
        scores = jnp.where(in_range, scores, masked_score)
        new_max = jnp.maximum(running_max, jnp.max(scores, axis=-1))
        rescale = jnp.exp(running_max - new_max)
        weights = jnp.exp(scores - new_max[..., None])
        weight_total = weight_total * rescale + jnp.sum(weights, axis=-1)
        weighted_sum = weighted_sum * rescale[..., None] + jnp.einsum(
            "shk,skc->shc",
            weights.astype(jnp.bfloat16),
            block_latent,
            preferred_element_type=jnp.float32,
        )
        return (new_max, weight_total, weighted_sum)

    longest = jnp.max(lengths)
    block_count = (longest + ABLK - 1) // ABLK
    ones_start = jnp.ones_like(new_score)
    sum_start = ones_start[..., None] * latent_new.astype(jnp.float32)[:, None, :]
    final_max, weight_total, weighted_sum = lax.fori_loop(
        0, block_count, attend_block, (new_score, ones_start, sum_start)
    )
    latent_out = (weighted_sum / weight_total[..., None]).astype(jnp.bfloat16)
    heads_out = (
        jnp.einsum("shc,chv->shv", latent_out, value_up, preferred_element_type=jnp.float32)
        .astype(jnp.bfloat16)
        .reshape(seq_count, -1)
    )
    column_rows = jnp.dot(
        lax.all_gather(heads_out, ("ep", "tp"), axis=0, tiled=True),
        out_proj,
        preferred_element_type=jnp.float32,
    ).astype(jnp.bfloat16)
    mixed_rows = lax.all_to_all(column_rows, ("ep", "tp"), split_axis=0, concat_axis=1, tiled=True)
    after_mix = (
        hidden_in.astype(jnp.float32)
        + gain_mix.astype(jnp.float32) * normalize(mixed_rows.astype(jnp.float32))
    ).astype(jnp.bfloat16)
    ffn_in = (normalize(after_mix.astype(jnp.float32)) * gain_ffn_in.astype(jnp.float32)).astype(
        jnp.bfloat16
    )
    affinity = jax.nn.sigmoid(jnp.dot(ffn_in, router, preferred_element_type=jnp.float32))
    experts_total = router.shape[1]
    own_start = lax.axis_index("tp") * seq_count
    own_routes = lax.dynamic_slice_in_dim(routes, own_start, seq_count, 0)
    choose = own_routes[..., None] == lax.iota(jnp.int32, experts_total)[None, None, :]
    chosen = jnp.sum(jnp.where(choose, affinity[:, None, :], 0.0), axis=-1)
    route_weights = chosen / jnp.sum(chosen, axis=-1, keepdims=True) * routed_scale
    group_rows, top_count = routes.shape
    capacity = 2 * ((group_rows * top_count + experts_total - 1) // experts_total)
    flat_routes = routes.reshape(-1)
    order_index = lax.iota(jnp.int32, group_rows * top_count)
    same_expert = flat_routes[:, None] == flat_routes[None, :]
    earlier = order_index[None, :] < order_index[:, None]
    slot_number = jnp.sum(jnp.logical_and(same_expert, earlier), axis=1)
    slot_number = slot_number.reshape(group_rows, top_count)
    own_slots = lax.dynamic_slice_in_dim(slot_number, own_start, seq_count, 0)
    slot_index = own_routes * capacity + own_slots
    slots_total = experts_total * capacity
    slot_table = jnp.any(
        slot_index[None, :, :] == lax.iota(jnp.int32, slots_total)[:, None, None], axis=-1
    ).astype(jnp.bfloat16)
    outgoing_terms = jnp.dot(slot_table, ffn_in, preferred_element_type=jnp.float32)
    outgoing = outgoing_terms.astype(jnp.bfloat16).reshape(experts_total, capacity, -1)
    received = lax.all_to_all(outgoing, ("ep", "tp"), split_axis=0, concat_axis=0, tiled=True)
    ep_count = lax.axis_size("ep")
    tp_count = lax.axis_size("tp")
    item_count = received.shape[1]
    width = received.shape[2]
    merged = jnp.sum(received.reshape(ep_count, tp_count, item_count, width), axis=1)
    outputs = swiglu(
        merged.reshape(ep_count * item_count, width), expert_gate[0], expert_up[0], expert_down[0]
    )
    copies = jnp.broadcast_to(
        outputs.reshape(ep_count, 1, item_count, width), (ep_count, tp_count, item_count, width)
    )
    copies = copies.reshape(ep_count * tp_count, item_count, width)
    returned = lax.all_to_all(copies, ("ep", "tp"), split_axis=0, concat_axis=0, tiled=True)
    picked = returned.reshape(slots_total, -1)[slot_index]
    routed = jnp.sum(picked.astype(jnp.float32) * route_weights[..., None], axis=1)
    shared = swiglu(ffn_in, shared_gate, shared_up, shared_down)
    combined = routed + shared.astype(jnp.float32)
    return (
        after_mix.astype(jnp.float32) + gain_ffn_out.astype(jnp.float32) * normalize(combined)
    ).astype(jnp.bfloat16)


def flip(index, mask, bits):
    result = 0
    for b in range(bits):
        bit = (index // 2**b) % 2
        result = result + (1 - bit if mask >> b & 1 else bit) * 2**b
    return result


def fused_kernel(
    ep_count,
    score_scale,
    hidden_hbm,
    qn_hbm,
    qr_hbm,
    nl_hbm,
    nr_hbm,
    len_hbm,
    routes_hbm,
    gm_hbm,
    gf_hbm,
    go_hbm,
    ab_hbm,
    cl_hbm,
    cr_hbm,
    vup_hbm,
    wo_hbm,
    router_hbm,
    eg_hbm,
    eu_hbm,
    ed_hbm,
    sg_hbm,
    su_hbm,
    sd_hbm,
    out_ref,
    hidden,
    qn,
    qr,
    nl,
    nr,
    length_of,
    route_of,
    gm,
    gf,
    go,
    ab,
    keys,
    rope_keys,
    vraw,
    wo,
    router,
    eg,
    eu,
    ed,
    sg,
    su,
    sd,
    vup,
    wq,
    new_keys,
    lat,
    xbuf,
    hbuf,
    cbuf,
    norm_rows,
    mix_rows,
    terms,
    back,
    local_sem,
    cache_sem,
    pair_send,
    pair_recv,
    ag_send,
    ag_recv,
):
    seq_count, heads, nope = qn.shape
    rope = qr.shape[2]
    width = out_ref.shape[1]
    latent = nl.shape[1]
    rows = seq_count * heads
    total_rows = ep_count * seq_count
    bits = (ep_count - 1).bit_length()
    me_e = lax.axis_index("ep")
    me_t = lax.axis_index("tp")

    def device(e, t):
        return {"ep": e, "tp": t}

    sibling = device(me_e, 1 - me_t)
    far_first = list(range(ep_count - 1, 0, -1))
    barrier = pltpu.get_barrier_semaphore()
    for target in [device(flip(me_e, mask, bits), me_t) for mask in far_first] + [sibling]:
        pl.semaphore_signal(
            barrier, inc=1, device_id=target, device_id_type=pl.DeviceIdType.MESH
        )

    started = []

    def fetch(source, target):
        copy = pltpu.make_async_copy(source, target, local_sem.at[len(started)])
        copy.start()
        started.append(copy)
        return copy

    len_copy = fetch(len_hbm, length_of)
    query_copies = [
        fetch(s, t) for s, t in ((qr_hbm, qr), (nl_hbm, nl), (nr_hbm, nr), (qn_hbm, qn))
    ]
    absorb_copy = fetch(ab_hbm, ab)
    value_copy = fetch(vup_hbm, vraw)
    rope_copy = fetch(cr_hbm, rope_keys)
    cache_copies = []
    for s in range(seq_count):
        copy = pltpu.make_async_copy(
            cl_hbm.at[s], keys.at[:, s * latent : (s + 1) * latent], cache_sem.at[s]
        )
        copy.start()
        cache_copies.append(copy)
    row_copies = [fetch(routes_hbm, route_of), fetch(hidden_hbm, hidden)]
    wo_copy = fetch(wo_hbm, wo.at[me_t])
    gain_copies = [fetch(s, t) for s, t in ((gm_hbm, gm), (gf_hbm, gf), (go_hbm, go))]
    router_copy = fetch(router_hbm, router)
    expert_copies = [
        fetch(s, t.at[me_t]) for s, t in ((eg_hbm, eg), (eu_hbm, eu), (ed_hbm, ed))
    ]
    shared_copies = [fetch(s, t) for s, t in ((sg_hbm, sg), (su_hbm, su), (sd_hbm, sd))]

    def to_sibling(index, source, target):
        return pltpu.make_async_remote_copy(
            src_ref=source,
            dst_ref=target.at[me_t],
            send_sem=pair_send.at[index],
            recv_sem=pair_recv.at[index],
            device_id=sibling,
            device_id_type=pl.DeviceIdType.MESH,
        )

    pair_copies = [
        to_sibling(index, source, target)
        for index, (source, target) in enumerate(
            ((wo_hbm, wo), (eg_hbm, eg), (eu_hbm, eu), (ed_hbm, ed))
        )
    ]

    value_dim = vraw.shape[2]
    step = 256 // heads
    order_row = lax.broadcasted_iota(jnp.int32, (256, 256), 0)
    order_lane = lax.broadcasted_iota(jnp.int32, (256, 256), 1)
    order = jnp.where(
        order_lane == order_row % step * heads + order_row // step, 1.0, 0.0
    ).astype(jnp.bfloat16)

    half = rope // 2
    turn_row = lax.broadcasted_iota(jnp.int32, (seq_count, rope), 0)
    turn_lane = lax.broadcasted_iota(jnp.int32, (seq_count, rope), 1)
    inverse = jnp.zeros((seq_count, rope), jnp.float32)
    for i in range(half):
        inverse = jnp.where(turn_lane % half == i, rope_theta ** (-2.0 * i / rope), inverse)
    len_copy.wait()
    position = jnp.zeros((seq_count, rope), jnp.float32)
    for s in range(seq_count):
        position = jnp.where(turn_row == s, length_of[s].astype(jnp.float32), position)
    angles = position * inverse
    cosine = jnp.cos(angles)
    sine = jnp.sin(angles) * jnp.where(turn_lane < half, -1.0, 1.0)

    def turned(values, cos_rows, sin_rows):
        swapped = jnp.concatenate([values[:, half:], values[:, :half]], axis=1)
        return values * cos_rows + swapped * sin_rows

    def per_head(table):
        return jnp.broadcast_to(table[:, None, :], (seq_count, heads, rope)).reshape(rows, rope)

    for copy in query_copies:
        copy.wait()
    query_rows = qr[...].astype(jnp.float32).reshape(rows, rope)
    q_pe = turned(query_rows, per_head(cosine), per_head(sine))
    key_rows = turned(nr[...].astype(jnp.float32), cosine, sine)
    new_rows = normalize(nl[...].astype(jnp.float32)).astype(jnp.bfloat16).astype(jnp.float32)
    rope_at = seq_count * latent
    new_keys[...] = jnp.zeros_like(new_keys)
    for s in range(seq_count):
        new_keys[0:1, s * latent : (s + 1) * latent] = new_rows[s : s + 1, :]
    new_keys[0:1, rope_at:] = jnp.concatenate(
        [key_rows[s : s + 1, :] for s in range(seq_count)], axis=1
    )

    nope_rows = qn[...].astype(jnp.float32).reshape(rows, nope)
    row_head = lax.broadcasted_iota(jnp.int32, (rows, 2 * nope), 0) % heads
    pair_lane = lax.broadcasted_iota(jnp.int32, (rows, 2 * nope), 1) // nope
    doubled = jnp.concatenate([nope_rows, nope_rows], axis=1)
    spread_query = jnp.concatenate(
        [
            jnp.where(row_head == pair_lane + 2 * j, doubled, 0.0).astype(jnp.bfloat16)
            for j in range(heads // 2)
        ],
        axis=1,
    )
    absorb_copy.wait()
    q_lat = jnp.dot(spread_query, ab[...], preferred_element_type=jnp.float32)
    q_turned = q_lat.T
    lane_seq = lax.broadcasted_iota(jnp.int32, (latent, rows), 1) // heads
    for s in range(seq_count):
        wq[s * latent : (s + 1) * latent, :] = jnp.where(lane_seq == s, q_turned, 0.0).astype(
            jnp.bfloat16
        )
    rope_turned = jnp.concatenate([q_pe] * (128 // rope), axis=1).T[:rope]
    rope_seq = lax.broadcasted_iota(jnp.int32, (rope, rows), 1) // heads
    for s in range(seq_count):
        wq[rope_at + s * rope : rope_at + (s + 1) * rope, :] = jnp.where(
            rope_seq == s, rope_turned, 0.0
        ).astype(jnp.bfloat16)

    value_copy.wait()
    for b in range(0, latent // step, 2):
        blocks = [
            vraw[i * step : (i + 1) * step].reshape(step * heads, value_dim) for i in (b, b + 1)
        ]
        ordered = jnp.dot(
            order, jnp.concatenate(blocks, axis=1), preferred_element_type=jnp.float32
        ).astype(jnp.bfloat16)
        for i in range(2):
            for h in range(heads):
                vup[(b + i) * step : (b + i + 1) * step, h * value_dim : (h + 1) * value_dim] = (
                    ordered[h * step : (h + 1) * step, i * value_dim : (i + 1) * value_dim]
                )

    context = keys.shape[0]
    rope_copy.wait()
    keys[:, rope_at:] = rope_keys[...].T
    for copy in cache_copies:
        copy.wait()
    lengths_row = jnp.zeros((1, rows), jnp.int32)
    lane_of = lax.broadcasted_iota(jnp.int32, (1, rows), 1) // heads
    for s in range(seq_count):
        lengths_row = jnp.where(lane_of == s, length_of[s], lengths_row)
    new_score = (
        jnp.dot(new_keys[...].astype(jnp.bfloat16), wq[...], preferred_element_type=jnp.float32)[
            0:1
        ]
        * score_scale
    )
    scores = jnp.dot(keys[...], wq[...], preferred_element_type=jnp.float32) * score_scale
    key_index = lax.broadcasted_iota(jnp.int32, (context, rows), 0)
    scores = jnp.where(key_index < lengths_row, scores, masked_score)
    row_max = jnp.maximum(jnp.max(scores, axis=0, keepdims=True), new_score)
    weights = jnp.exp(scores - row_max)
    new_weight = jnp.exp(new_score - row_max)
    weight_total = jnp.sum(weights, axis=0, keepdims=True) + new_weight
    new_weight = new_weight.astype(jnp.bfloat16).astype(jnp.float32)
    turned_weights = weights.astype(jnp.bfloat16).T
    side = jnp.concatenate(
        [weight_total, new_weight, jnp.zeros((6, rows), jnp.float32)], axis=0
    ).T
    for s in range(seq_count):
        part = slice(s * heads, (s + 1) * heads)
        weighted = jnp.dot(
            turned_weights[part],
            keys[:, s * latent : (s + 1) * latent],
            preferred_element_type=jnp.float32,
        )
        weighted = weighted + side[part, 1:2] * new_rows[s : s + 1, :]
        lat[part, :] = (weighted / side[part, 0:1]).astype(jnp.bfloat16)

    spread = jnp.dot(lat[...], vup[...], preferred_element_type=jnp.float32)
    own_heads = []
    head_row = lax.broadcasted_iota(jnp.int32, (seq_count, heads, value_dim), 1)
    for h in range(heads):
        block = spread[:, h * value_dim : (h + 1) * value_dim].reshape(seq_count, heads, value_dim)
        own_heads.append(jnp.sum(jnp.where(head_row == h, block, 0.0), axis=1))
    hbuf[me_e] = jnp.concatenate(own_heads, axis=1).astype(jnp.bfloat16)

    for copy in row_copies:
        copy.wait()
    xbuf[me_e, :, 0:width] = hidden[...]
    mark_shape = (seq_count, xbuf.shape[2] - width)
    mark_row = lax.broadcasted_iota(jnp.int32, mark_shape, 0)
    mark_lane = lax.broadcasted_iota(jnp.int32, mark_shape, 1)
    marks = jnp.zeros(mark_shape, jnp.float32)
    for s in range(seq_count):
        for j in range(route_of.shape[0]):
            expert = route_of[j, me_t * seq_count + s]
            marks = jnp.where((mark_row == s) & (mark_lane == expert), 1.0, marks)
    xbuf[me_e, :, width:] = marks.astype(jnp.bfloat16)

    pending = []

    def remote(which, mask, source, target, to):
        return pltpu.make_async_remote_copy(
            src_ref=source,
            dst_ref=target,
            send_sem=ag_send.at[which, mask],
            recv_sem=ag_recv.at[which, to],
            device_id=device(flip(me_e, mask, bits), me_t),
            device_id_type=pl.DeviceIdType.MESH,
        )

    def share(which, buf):
        for mask in far_first:
            copy = remote(which, mask, buf.at[me_e], buf.at[me_e], me_e)
            copy.start()
            pending.append(copy)

    def arrive(which, buf, mask):
        e = flip(me_e, mask, bits)
        remote(which, mask, buf.at[e], buf.at[e], e).wait_recv()

    pl.semaphore_wait(barrier, ep_count)
    share(1, hbuf)
    share(0, xbuf)
    for copy in pair_copies:
        copy.start()
    wo_copy.wait()
    pair_copies[0].wait_recv()
    for mask in reversed(far_first):
        arrive(1, hbuf, mask)

    flat_heads = hbuf[...].reshape(total_rows, hbuf.shape[2])
    cbuf[me_e] = jnp.concatenate(
        [jnp.dot(flat_heads, wo[t], preferred_element_type=jnp.float32) for t in range(2)], axis=1
    ).astype(jnp.bfloat16)
    share(2, cbuf)
    for mask in reversed(far_first):
        arrive(0, xbuf, mask)
    for copy in gain_copies + [router_copy] + expert_copies:
        copy.wait()
    for copy in pair_copies[1:]:
        copy.wait_recv()
    for mask in reversed(far_first):
        arrive(2, cbuf, mask)

    gains = [ref[...].astype(jnp.float32).reshape(1, width) for ref in (gm, gf, go)]
    mixed = jnp.concatenate([cbuf[o] for o in range(ep_count)], axis=1).astype(jnp.float32)
    stage = xbuf[...].reshape(total_rows, xbuf.shape[2])
    after_mix = (stage[:, :width].astype(jnp.float32) + gains[0] * normalize(mixed)).astype(
        jnp.bfloat16
    )
    mix_rows[...] = after_mix.reshape(mix_rows.shape)
    ffn_in = (normalize(after_mix.astype(jnp.float32)) * gains[1]).astype(jnp.bfloat16)
    norm_rows[...] = ffn_in.reshape(norm_rows.shape)
    affinity = jax.nn.sigmoid(
        lax.dot_general(
            ffn_in, router[...], (((1,), (1,)), ((), ())), preferred_element_type=jnp.float32
        )
    )
    hot = stage[:, width : width + affinity.shape[1]].astype(jnp.float32)
    chosen = affinity * hot
    lane = lax.broadcasted_iota(jnp.int32, chosen.shape, 1)
    whole = jnp.sum(chosen, axis=1, keepdims=True)
    outcome = jnp.zeros((total_rows, width), jnp.float32)
    for t in range(2):
        mine = jnp.sum(jnp.where(lane == me_e * 2 + t, chosen, 0.0), axis=1, keepdims=True)
        mine = mine / whole * routed_scale
        expert_out = swiglu(ffn_in, eg[t], eu[t], ed[t])
        outcome = outcome + expert_out.astype(jnp.float32) * mine
    terms[...] = outcome.astype(jnp.bfloat16).reshape(terms.shape)
    for mask in far_first:
        copy = remote(3, mask, terms.at[flip(me_e, mask, bits)], back.at[me_e], me_e)
        copy.start()
        pending.append(copy)
    for copy in shared_copies:
        copy.wait()
    combined = terms[me_e].astype(jnp.float32) + swiglu(
        norm_rows[me_e], sg[...], su[...], sd[...]
    ).astype(jnp.float32)
    for mask in reversed(far_first):
        arrive(3, back, mask)
        combined = combined + back[flip(me_e, mask, bits)].astype(jnp.float32)
    out_ref[...] = (
        mix_rows[me_e].astype(jnp.float32) + gains[2] * normalize(combined)
    ).astype(jnp.bfloat16)
    for copy in pending + pair_copies:
        copy.wait_send()


def local_fused(
    hidden_in,
    query_nope,
    query_rope,
    new_latent,
    new_rope,
    cache_latent,
    cache_rope,
    lengths,
    absorb_key,
    value_up,
    out_proj,
    gain_mix,
    gain_ffn_in,
    router,
    routes,
    expert_gate,
    expert_up,
    expert_down,
    shared_gate,
    shared_up,
    shared_down,
    gain_ffn_out,
):
    seq_count, width = hidden_in.shape
    heads, latent = query_nope.shape[1], cache_latent.shape[2]
    context, rope = cache_rope.shape[1:]
    ep_count = lax.axis_size("ep")
    bf = jnp.bfloat16
    score_scale = (query_nope.shape[-1] + query_rope.shape[-1]) ** (-0.5)
    dma = pltpu.SemaphoreType.DMA
    total_rows = ep_count * seq_count
    rows = seq_count * heads
    depth = seq_count * (latent + rope)
    rope_rows = jnp.swapaxes(cache_rope, 1, 2).reshape(seq_count * rope, context)
    router_rows = jnp.swapaxes(router, 0, 1)
    absorb_rows = jnp.transpose(absorb_key, (1, 2, 0)).reshape(-1, latent)
    route_rows = jnp.swapaxes(routes, 0, 1)
    gate, up, down = expert_gate[0], expert_up[0], expert_down[0]
    operands = (
        hidden_in,
        query_nope,
        query_rope,
        new_latent,
        new_rope,
        lengths,
        route_rows,
        gain_mix,
        gain_ffn_in,
        gain_ffn_out,
        absorb_rows,
        cache_latent,
        rope_rows,
        value_up,
        out_proj,
        router_rows,
        gate,
        up,
        down,
        shared_gate,
        shared_up,
        shared_down,
    )

    def near(array, lead=()):
        return pltpu.VMEM(lead + array.shape, array.dtype)

    flops = 2 * total_rows * width * out_proj.shape[1]
    return pl.pallas_call(
        functools.partial(fused_kernel, ep_count, score_scale),
        out_shape=jax.ShapeDtypeStruct((seq_count, width), bf),
        in_specs=[pl.BlockSpec(memory_space=pl.ANY)] * len(operands),
        out_specs=pl.BlockSpec(memory_space=pltpu.VMEM),
        scratch_shapes=[near(a) for a in operands[:5]]
        + [pltpu.SMEM(lengths.shape, jnp.int32), pltpu.SMEM(route_rows.shape, jnp.int32)]
        + [near(a) for a in operands[7:11]]
        + [
            pltpu.VMEM((context, depth), bf),
            near(rope_rows),
            near(value_up),
            near(out_proj, (2,)),
            near(router_rows),
            near(gate, (2,)),
            near(up, (2,)),
            near(down, (2,)),
            near(shared_gate),
            near(shared_up),
            near(shared_down),
            pltpu.VMEM((latent, heads * value_up.shape[2]), bf),
            pltpu.VMEM((depth, rows), bf),
            pltpu.VMEM((8, depth), jnp.float32),
            pltpu.VMEM((rows, latent), bf),
            pltpu.VMEM((ep_count, seq_count, width + 128), bf),
            pltpu.VMEM((ep_count, seq_count, out_proj.shape[0]), bf),
            pltpu.VMEM((ep_count, total_rows, 2 * out_proj.shape[1]), bf),
            pltpu.VMEM((ep_count, seq_count, width), bf),
            pltpu.VMEM((ep_count, seq_count, width), bf),
            pltpu.VMEM((ep_count, seq_count, width), bf),
            pltpu.VMEM((ep_count, seq_count, width), bf),
            dma((len(operands),)),
            dma((seq_count,)),
            dma((4,)),
            dma((4,)),
            dma((4, ep_count)),
            dma((4, ep_count)),
        ],
        compiler_params=pltpu.CompilerParams(
            collective_id=0, has_side_effects=True, vmem_limit_bytes=56 * 2**20
        ),
        cost_estimate=pl.CostEstimate(flops=flops, bytes_accessed=2**24, transcendentals=0),
        name="layer_step",
    )(*operands)


def local(*args):
    hidden_in, out_proj, router = args[0], args[10], args[13]
    device_count = lax.axis_size("ep") * lax.axis_size("tp")
    ep_count = lax.axis_size("ep")
    fits = (
        lax.axis_size("tp") == 2
        and ep_count & (ep_count - 1) == 0
        and hidden_in.shape[0] == 8
        and args[1].shape[1] == 16
        and device_count * hidden_in.shape[0] <= 256
        and out_proj.shape[1] % 128 == 0
        and router.shape[1] == device_count
    )
    return local_fused(*args) if fits else local_wide(*args)


def solution(mesh):
    placed = (
        P(("grp", "ep", "tp"), None),
        P(("grp", "ep", "tp"), None, None),
        P(("grp", "ep", "tp"), None, None),
        P(("grp", "ep", "tp"), None),
        P(("grp", "ep", "tp"), None),
        P(("grp", "ep", "tp"), None, None),
        P(("grp", "ep", "tp"), None, None),
        P(("grp", "ep", "tp")),
        P(),
        P(),
        P(None, ("ep", "tp")),
        P(),
        P(),
        P(),
        P(("grp", "ep"), None),
        P(("ep", "tp"), None, None),
        P(("ep", "tp"), None, None),
        P(("ep", "tp"), None, None),
        P(),
        P(),
        P(),
        P(),
    )
    return jax.shard_map(
        local, mesh=mesh, in_specs=placed, out_specs=P(("grp", "ep", "tp"), None), check_vma=False
    )
```

time: 47.2 us -> 41.7 us (0.88)
  Pallas kernels: 45.6 us -> 40.2 us
    pallas_call x1, Pallas kernels: 45.6 us -> 40.2 us  [local_fused(): pl.pallas_call(functools.partial(fused_kernel, ep_count, score_scale), ou...]
where the time goes in v1:
time: 41.7 us; the launch traced here: 41.6 us
  Pallas kernels  40.2 us (96%)
  local copies, waits for them, and re-layouts  1.38 us (3%)
    pallas_call x1, Pallas kernels, local_fused(): pl.pallas_call(functools.partial(fused_kernel, ep_count, score_scale), ou...  40.2 us
    unnamed x1, local copies, waits for them, and re-layouts  1.38 us

profile of v1, /device:TPU:0, one launch (start us, length us, event | category | flops | bytes accessed | tf_op | source)
XLA Modules:
  0.0 41.6 jit_solution(15823825435671402583)
XLA Ops:
  0.0 40.2 %layer_step.1 = bf16[8,2048]{1,0:T(8,128)(2,1)} custom-call(bf16[8,2048]{1,0:T(8,128)(2,1)} %hidden_hbm.1, bf16[8,16,64]{2,1,0:T(8,128)(2,1)} %qn_hbm.1, bf16[8,16,32]{2,1,0:T(8,128)(2,1)} %qr_hbm.1, bf16[8,256]{1,0:T(8,128)(2,1)} %nl_hbm.1, bf16[8,32]{1,0:T(8,128)(2,1)} %nr_hbm.1, s32[8]{0:T(128)} %len_hbm.1, s32[6,16]{1,0:T(8,128)} %bitcast.17, ...), custom_call_target="tpu_custom_call" | custom-call | flops 33554432 | bytes 16777216 | tf_op jit(solution)/shard_map/layer_step/pallas_call | solution.py:625
  40.2 1.4 %copy.24 = bf16[8,2048]{1,0:T(8,128)(2,1)} copy(bf16[8,2048]{1,0:T(8,128)(2,1)} %layer_step.1) | data formatting | bytes 65536

commit v2 on v1

--- a/solution.py
+++ b/solution.py
@@ -1,4 +1,5 @@
 import functools
+import math
 
 import jax
 import jax.numpy as jnp
@@ -253,6 +254,9 @@
     pair_recv,
     ag_send,
     ag_recv,
+    ready,
+    scores,
+    turned_weights,
 ):
     seq_count, heads, nope = qn.shape
     rope = qr.shape[2]
@@ -270,10 +274,15 @@
     sibling = device(me_e, 1 - me_t)
     far_first = list(range(ep_count - 1, 0, -1))
     barrier = pltpu.get_barrier_semaphore()
-    for target in [device(flip(me_e, mask, bits), me_t) for mask in far_first] + [sibling]:
+
+    def tell(semaphore, target):
         pl.semaphore_signal(
-            barrier, inc=1, device_id=target, device_id_type=pl.DeviceIdType.MESH
-        )
+            semaphore, inc=1, device_id=target, device_id_type=pl.DeviceIdType.MESH
+        )
+
+    @pl.when(me_t == 1)
+    def _():
+        tell(barrier, sibling)
 
     started = []
 
@@ -297,15 +306,6 @@
         )
         copy.start()
         cache_copies.append(copy)
-    row_copies = [fetch(routes_hbm, route_of), fetch(hidden_hbm, hidden)]
-    wo_copy = fetch(wo_hbm, wo.at[me_t])
-    gain_copies = [fetch(s, t) for s, t in ((gm_hbm, gm), (gf_hbm, gf), (go_hbm, go))]
-    router_copy = fetch(router_hbm, router)
-    expert_copies = [
-        fetch(s, t.at[me_t]) for s, t in ((eg_hbm, eg), (eu_hbm, eu), (ed_hbm, ed))
-    ]
-    shared_copies = [fetch(s, t) for s, t in ((sg_hbm, sg), (su_hbm, su), (sd_hbm, sd))]
-
     def to_sibling(index, source, target):
         return pltpu.make_async_remote_copy(
             src_ref=source,
@@ -322,6 +322,20 @@
             ((wo_hbm, wo), (eg_hbm, eg), (eu_hbm, eu), (ed_hbm, ed))
         )
     ]
+
+    @pl.when(me_t == 0)
+    def _():
+        pl.semaphore_wait(barrier, 1)
+        tell(ready.at[0], sibling)
+
+    @pl.when(me_t == 1)
+    def _():
+        pl.semaphore_wait(ready.at[0], 1)
+        for mask in far_first:
+            tell(barrier, device(flip(me_e, mask, bits), me_t))
+
+    for copy in pair_copies:
+        copy.start()
 
     value_dim = vraw.shape[2]
     step = 256 // heads
@@ -409,34 +423,49 @@
     context = keys.shape[0]
     rope_copy.wait()
     keys[:, rope_at:] = rope_keys[...].T
-    for copy in cache_copies:
-        copy.wait()
     lengths_row = jnp.zeros((1, rows), jnp.int32)
     lane_of = lax.broadcasted_iota(jnp.int32, (1, rows), 1) // heads
     for s in range(seq_count):
         lengths_row = jnp.where(lane_of == s, length_of[s], lengths_row)
-    new_score = (
-        jnp.dot(new_keys[...].astype(jnp.bfloat16), wq[...], preferred_element_type=jnp.float32)[
-            0:1
-        ]
-        * score_scale
-    )
-    scores = jnp.dot(keys[...], wq[...], preferred_element_type=jnp.float32) * score_scale
-    key_index = lax.broadcasted_iota(jnp.int32, (context, rows), 0)
-    scores = jnp.where(key_index < lengths_row, scores, masked_score)
-    row_max = jnp.maximum(jnp.max(scores, axis=0, keepdims=True), new_score)
-    weights = jnp.exp(scores - row_max)
-    new_weight = jnp.exp(new_score - row_max)
-    weight_total = jnp.sum(weights, axis=0, keepdims=True) + new_weight
+    new_score = jnp.dot(
+        new_keys[...].astype(jnp.bfloat16), wq[...], preferred_element_type=jnp.float32
+    )[0:1]
+    for copy in cache_copies:
+        copy.wait()
+    row_copies = [fetch(routes_hbm, route_of), fetch(hidden_hbm, hidden)]
+    wo_copy = fetch(wo_hbm, wo.at[me_t])
+    gain_copies = [fetch(s, t) for s, t in ((gm_hbm, gm), (gf_hbm, gf), (go_hbm, go))]
+    router_copy = fetch(router_hbm, router)
+    expert_copies = [
+        fetch(s, t.at[me_t]) for s, t in ((eg_hbm, eg), (eu_hbm, eu), (ed_hbm, ed))
+    ]
+    shared_copies = [fetch(s, t) for s, t in ((sg_hbm, sg), (su_hbm, su), (sd_hbm, sd))]
+
+    block = 256
+    key_index = lax.broadcasted_iota(jnp.int32, (block, rows), 0)
+    tops = jnp.full((8, rows), masked_score, jnp.float32)
+    for k in range(0, context, block):
+        found = jnp.dot(keys[k : k + block, :], wq[...], preferred_element_type=jnp.float32)
+        found = jnp.where(key_index < lengths_row - k, found, masked_score)
+        scores[k : k + block, :] = found
+        tops = jnp.maximum(tops, jnp.max(found.reshape(block // 8, 8, rows), axis=0))
+    row_max = jnp.maximum(jnp.max(tops, axis=0, keepdims=True), new_score)
+    power = score_scale * math.log2(math.e)
+    sums = jnp.zeros((8, rows), jnp.float32)
+    for k in range(0, context, block):
+        weights = jnp.exp2((scores[k : k + block, :] - row_max) * power)
+        sums = sums + jnp.sum(weights.reshape(block // 8, 8, rows), axis=0)
+        turned_weights[:, k : k + block] = weights.astype(jnp.bfloat16).T
+    new_weight = jnp.exp2((new_score - row_max) * power)
+    weight_total = jnp.sum(sums, axis=0, keepdims=True) + new_weight
     new_weight = new_weight.astype(jnp.bfloat16).astype(jnp.float32)
-    turned_weights = weights.astype(jnp.bfloat16).T
     side = jnp.concatenate(
         [weight_total, new_weight, jnp.zeros((6, rows), jnp.float32)], axis=0
     ).T
     for s in range(seq_count):
         part = slice(s * heads, (s + 1) * heads)
         weighted = jnp.dot(
-            turned_weights[part],
+            turned_weights[part, :],
             keys[:, s * latent : (s + 1) * latent],
             preferred_element_type=jnp.float32,
         )
@@ -486,11 +515,17 @@
         e = flip(me_e, mask, bits)
         remote(which, mask, buf.at[e], buf.at[e], e).wait_recv()
 
-    pl.semaphore_wait(barrier, ep_count)
+    @pl.when(me_t == 1)
+    def _():
+        pl.semaphore_wait(barrier, ep_count - 1)
+        tell(ready.at[1], sibling)
+
+    @pl.when(me_t == 0)
+    def _():
+        pl.semaphore_wait(ready.at[1], 1)
+
     share(1, hbuf)
     share(0, xbuf)
-    for copy in pair_copies:
-        copy.start()
     wo_copy.wait()
     pair_copies[0].wait_recv()
     for mask in reversed(far_first):
@@ -624,7 +659,7 @@
     flops = 2 * total_rows * width * out_proj.shape[1]
     return pl.pallas_call(
         functools.partial(fused_kernel, ep_count, score_scale),
-        out_shape=jax.ShapeDtypeStruct((seq_count, width), bf),
+        out_shape=pltpu.VMEM((seq_count, width), bf),
         in_specs=[pl.BlockSpec(memory_space=pl.ANY)] * len(operands),
         out_specs=pl.BlockSpec(memory_space=pltpu.VMEM),
         scratch_shapes=[near(a) for a in operands[:5]]
@@ -659,6 +694,9 @@
             dma((4,)),
             dma((4, ep_count)),
             dma((4, ep_count)),
+            pltpu.SemaphoreType.REGULAR((2,)),
+            pltpu.VMEM((context, rows), jnp.float32),
+            pltpu.VMEM((rows, context), bf),
         ],
         compiler_params=pltpu.CompilerParams(
             collective_id=0, has_side_effects=True, vmem_limit_bytes=56 * 2**20

time: 41.7 us -> 36.8 us (0.88)
  Pallas kernels: 40.2 us -> 36 us
  local copies, waits for them, and re-layouts: 1.38 us -> 0.62 us
    pallas_call x1, Pallas kernels: 40.2 us -> 36 us  [local_fused(): pl.pallas_call(functools.partial(fused_kernel, ep_count, score_scale), ou...]
    unnamed x1, local copies, waits for them, and re-layouts: 1.38 us -> 0.62 us
where the time goes in v2:
time: 36.8 us; the launch traced here: 36.6 us
  Pallas kernels  36 us (98%)
  local copies, waits for them, and re-layouts  0.62 us (2%)
    pallas_call x1, Pallas kernels, local_fused(): pl.pallas_call(functools.partial(fused_kernel, ep_count, score_scale), ou...  36 us

profile of v2, /device:TPU:0, one launch (start us, length us, event | category | flops | bytes accessed | tf_op | source)
XLA Modules:
  0.0 36.6 jit_solution(9905716839572600219)
XLA Ops:
  0.0 36.0 %layer_step.1 = bf16[8,2048]{1,0:T(8,128)(2,1)S(1)} custom-call(bf16[8,2048]{1,0:T(8,128)(2,1)} %hidden_hbm.1, bf16[8,16,64]{2,1,0:T(8,128)(2,1)} %qn_hbm.1, bf16[8,16,32]{2,1,0:T(8,128)(2,1)} %qr_hbm.1, bf16[8,256]{1,0:T(8,128)(2,1)} %nl_hbm.1, bf16[8,32]{1,0:T(8,128)(2,1)} %nr_hbm.1, s32[8]{0:T(128)} %len_hbm.1, s32[6,16]{1,0:T(8,128)} %bitcast.17, ...), custom_call_target="tpu_custom_call" | custom-call | flops 33554432 | bytes 16777216 | tf_op jit(solution)/shard_map/layer_step/pallas_call | solution.py:660
  36.0 0.6 %copy.24 = bf16[8,2048]{1,0:T(8,128)(2,1)} copy(bf16[8,2048]{1,0:T(8,128)(2,1)S(1)} %layer_step.1) | data formatting | bytes 65536

commit v3 on v2

--- a/solution.py
+++ b/solution.py
@@ -231,15 +231,15 @@
     vraw,
     wo,
     router,
-    eg,
-    eu,
+    egu,
     ed,
-    sg,
-    su,
+    sgu,
     sd,
     vup,
     wq,
     new_keys,
+    scores,
+    turned_weights,
     lat,
     xbuf,
     hbuf,
@@ -249,21 +249,20 @@
     terms,
     back,
     local_sem,
-    cache_sem,
     pair_send,
     pair_recv,
-    ag_send,
-    ag_recv,
+    far_send,
+    far_recv,
     ready,
-    scores,
-    turned_weights,
 ):
     seq_count, heads, nope = qn.shape
     rope = qr.shape[2]
     width = out_ref.shape[1]
     latent = nl.shape[1]
     rows = seq_count * heads
-    total_rows = ep_count * seq_count
+    chunks, _, unit, _ = hbuf.shape
+    chunk_rows = ep_count * unit
+    chunk_depth = unit * (latent + rope)
     bits = (ep_count - 1).bit_length()
     me_e = lax.axis_index("ep")
     me_t = lax.axis_index("tp")
@@ -284,13 +283,15 @@
     def _():
         tell(barrier, sibling)
 
-    started = []
-
-    def fetch(source, target):
-        copy = pltpu.make_async_copy(source, target, local_sem.at[len(started)])
+    sems = iter(range(local_sem.shape[0]))
+
+    def fetch(source, target, sem=None):
+        copy = pltpu.make_async_copy(source, target, local_sem.at[next(sems) if sem is None else sem])
         copy.start()
-        started.append(copy)
         return copy
+
+    def all_of(region, sem):
+        return pltpu.make_async_copy(region, region, local_sem.at[sem])
 
     len_copy = fetch(len_hbm, length_of)
     query_copies = [
@@ -298,18 +299,21 @@
     ]
     absorb_copy = fetch(ab_hbm, ab)
     value_copy = fetch(vup_hbm, vraw)
+    row_copies = [fetch(routes_hbm, route_of), fetch(hidden_hbm, hidden)]
     rope_copy = fetch(cr_hbm, rope_keys)
     cache_copies = []
-    for s in range(seq_count):
-        copy = pltpu.make_async_copy(
-            cl_hbm.at[s], keys.at[:, s * latent : (s + 1) * latent], cache_sem.at[s]
-        )
-        copy.start()
-        cache_copies.append(copy)
+    for c in range(chunks):
+        sem = next(sems)
+        for i in range(unit):
+            at = c * chunk_depth + i * latent
+            fetch(cl_hbm.at[c * unit + i], keys.at[:, at : at + latent], sem)
+        at = c * chunk_depth
+        cache_copies.append(all_of(keys.at[:, at : at + unit * latent], sem))
+
     def to_sibling(index, source, target):
         return pltpu.make_async_remote_copy(
             src_ref=source,
-            dst_ref=target.at[me_t],
+            dst_ref=target,
             send_sem=pair_send.at[index],
             recv_sem=pair_recv.at[index],
             device_id=sibling,
@@ -319,7 +323,12 @@
     pair_copies = [
         to_sibling(index, source, target)
         for index, (source, target) in enumerate(
-            ((wo_hbm, wo), (eg_hbm, eg), (eu_hbm, eu), (ed_hbm, ed))
+            (
+                (wo_hbm, wo.at[me_t]),
+                (eg_hbm, egu.at[me_t, 0]),
+                (eu_hbm, egu.at[me_t, 1]),
+                (ed_hbm, ed.at[me_t]),
+            )
         )
     ]
 
@@ -372,13 +381,21 @@
     q_pe = turned(query_rows, per_head(cosine), per_head(sine))
     key_rows = turned(nr[...].astype(jnp.float32), cosine, sine)
     new_rows = normalize(nl[...].astype(jnp.float32)).astype(jnp.bfloat16).astype(jnp.float32)
-    rope_at = seq_count * latent
+
+    def places(s):
+        base = s // unit * chunk_depth
+        at = base + s % unit * latent
+        rope_at = base + unit * latent + s % unit * rope
+        return slice(at, at + latent), slice(rope_at, rope_at + rope)
+
     new_keys[...] = jnp.zeros_like(new_keys)
     for s in range(seq_count):
-        new_keys[0:1, s * latent : (s + 1) * latent] = new_rows[s : s + 1, :]
-    new_keys[0:1, rope_at:] = jnp.concatenate(
-        [key_rows[s : s + 1, :] for s in range(seq_count)], axis=1
-    )
+        new_keys[0:1, places(s)[0]] = new_rows[s : s + 1, :]
+    for c in range(chunks):
+        at = c * chunk_depth + unit * latent
+        new_keys[0:1, at : at + unit * rope] = jnp.concatenate(
+            [key_rows[s : s + 1, :] for s in range(c * unit, (c + 1) * unit)], axis=1
+        )
 
     nope_rows = qn[...].astype(jnp.float32).reshape(rows, nope)
     row_head = lax.broadcasted_iota(jnp.int32, (rows, 2 * nope), 0) % heads
@@ -395,16 +412,12 @@
     q_lat = jnp.dot(spread_query, ab[...], preferred_element_type=jnp.float32)
     q_turned = q_lat.T
     lane_seq = lax.broadcasted_iota(jnp.int32, (latent, rows), 1) // heads
-    for s in range(seq_count):
-        wq[s * latent : (s + 1) * latent, :] = jnp.where(lane_seq == s, q_turned, 0.0).astype(
-            jnp.bfloat16
-        )
     rope_turned = jnp.concatenate([q_pe] * (128 // rope), axis=1).T[:rope]
     rope_seq = lax.broadcasted_iota(jnp.int32, (rope, rows), 1) // heads
     for s in range(seq_count):
-        wq[rope_at + s * rope : rope_at + (s + 1) * rope, :] = jnp.where(
-            rope_seq == s, rope_turned, 0.0
-        ).astype(jnp.bfloat16)
+        place, rope_place = places(s)
+        wq[place, :] = jnp.where(lane_seq == s, q_turned, 0.0).astype(jnp.bfloat16)
+        wq[rope_place, :] = jnp.where(rope_seq == s, rope_turned, 0.0).astype(jnp.bfloat16)
 
     value_copy.wait()
     for b in range(0, latent // step, 2):
@@ -420,9 +433,23 @@
                     ordered[h * step : (h + 1) * step, i * value_dim : (i + 1) * value_dim]
                 )
 
+    for copy in row_copies:
+        copy.wait()
+    mark_shape = (seq_count, xbuf.shape[3] - width)
+    mark_row = lax.broadcasted_iota(jnp.int32, mark_shape, 0)
+    mark_lane = lax.broadcasted_iota(jnp.int32, mark_shape, 1)
+    marks = jnp.zeros(mark_shape, jnp.float32)
+    for s in range(seq_count):
+        for j in range(route_of.shape[0]):
+            expert = route_of[j, me_t * seq_count + s]
+            marks = jnp.where((mark_row == s) & (mark_lane == expert), 1.0, marks)
+    own_rows = hidden[...].astype(jnp.float32)
+    for c in range(chunks):
+        part = slice(c * unit, (c + 1) * unit)
+        xbuf[me_e, c, :, 0:width] = own_rows[part].astype(jnp.bfloat16)
+        xbuf[me_e, c, :, width:] = marks[part].astype(jnp.bfloat16)
+
     context = keys.shape[0]
-    rope_copy.wait()
-    keys[:, rope_at:] = rope_keys[...].T
     lengths_row = jnp.zeros((1, rows), jnp.int32)
     lane_of = lax.broadcasted_iota(jnp.int32, (1, rows), 1) // heads
     for s in range(seq_count):
@@ -430,90 +457,120 @@
     new_score = jnp.dot(
         new_keys[...].astype(jnp.bfloat16), wq[...], preferred_element_type=jnp.float32
     )[0:1]
-    for copy in cache_copies:
-        copy.wait()
-    row_copies = [fetch(routes_hbm, route_of), fetch(hidden_hbm, hidden)]
-    wo_copy = fetch(wo_hbm, wo.at[me_t])
-    gain_copies = [fetch(s, t) for s, t in ((gm_hbm, gm), (gf_hbm, gf), (go_hbm, go))]
-    router_copy = fetch(router_hbm, router)
-    expert_copies = [
-        fetch(s, t.at[me_t]) for s, t in ((eg_hbm, eg), (eu_hbm, eu), (ed_hbm, ed))
-    ]
-    shared_copies = [fetch(s, t) for s, t in ((sg_hbm, sg), (su_hbm, su), (sd_hbm, sd))]
+    rope_copy.wait()
+    for c in range(chunks):
+        at = c * chunk_depth + unit * latent
+        keys[:, at : at + unit * rope] = rope_keys[c * unit * rope : (c + 1) * unit * rope].T
 
     block = 256
     key_index = lax.broadcasted_iota(jnp.int32, (block, rows), 0)
-    tops = jnp.full((8, rows), masked_score, jnp.float32)
-    for k in range(0, context, block):
-        found = jnp.dot(keys[k : k + block, :], wq[...], preferred_element_type=jnp.float32)
-        found = jnp.where(key_index < lengths_row - k, found, masked_score)
-        scores[k : k + block, :] = found
-        tops = jnp.maximum(tops, jnp.max(found.reshape(block // 8, 8, rows), axis=0))
-    row_max = jnp.maximum(jnp.max(tops, axis=0, keepdims=True), new_score)
     power = score_scale * math.log2(math.e)
-    sums = jnp.zeros((8, rows), jnp.float32)
-    for k in range(0, context, block):
-        weights = jnp.exp2((scores[k : k + block, :] - row_max) * power)
-        sums = sums + jnp.sum(weights.reshape(block // 8, 8, rows), axis=0)
-        turned_weights[:, k : k + block] = weights.astype(jnp.bfloat16).T
-    new_weight = jnp.exp2((new_score - row_max) * power)
-    weight_total = jnp.sum(sums, axis=0, keepdims=True) + new_weight
-    new_weight = new_weight.astype(jnp.bfloat16).astype(jnp.float32)
-    side = jnp.concatenate(
-        [weight_total, new_weight, jnp.zeros((6, rows), jnp.float32)], axis=0
-    ).T
-    for s in range(seq_count):
-        part = slice(s * heads, (s + 1) * heads)
-        weighted = jnp.dot(
-            turned_weights[part, :],
-            keys[:, s * latent : (s + 1) * latent],
+
+    def attend(c):
+        deep = slice(c * chunk_depth, (c + 1) * chunk_depth)
+        query = wq[deep, :]
+        tops = jnp.full((8, rows), masked_score, jnp.float32)
+        for k in range(0, context, block):
+            found = jnp.dot(keys[k : k + block, deep], query, preferred_element_type=jnp.float32)
+            found = jnp.where(key_index < lengths_row - k, found, masked_score)
+            scores[k : k + block, :] = found
+            tops = jnp.maximum(tops, jnp.max(found.reshape(block // 8, 8, rows), axis=0))
+        row_max = jnp.maximum(jnp.max(tops, axis=0, keepdims=True), new_score)
+        sums = jnp.zeros((8, rows), jnp.float32)
+        for k in range(0, context, block):
+            weights = jnp.exp2((scores[k : k + block, :] - row_max) * power)
+            sums = sums + jnp.sum(weights.reshape(block // 8, 8, rows), axis=0)
+            turned_weights[:, k : k + block] = weights.astype(jnp.bfloat16).T
+        new_weight = jnp.exp2((new_score - row_max) * power)
+        weight_total = jnp.sum(sums, axis=0, keepdims=True) + new_weight
+        new_weight = new_weight.astype(jnp.bfloat16).astype(jnp.float32)
+        side = jnp.concatenate(
+            [weight_total, new_weight, jnp.zeros((6, rows), jnp.float32)], axis=0
+        ).T
+        for s in range(c * unit, (c + 1) * unit):
+            part = slice(s * heads, (s + 1) * heads)
+            weighted = jnp.dot(
+                turned_weights[part, :], keys[:, places(s)[0]], preferred_element_type=jnp.float32
+            )
+            weighted = weighted + side[part, 1:2] * new_rows[s : s + 1, :]
+            lat[part, :] = (weighted / side[part, 0:1]).astype(jnp.bfloat16)
+        spread = jnp.dot(
+            lat[c * unit * heads : (c + 1) * unit * heads, :],
+            vup[...],
             preferred_element_type=jnp.float32,
         )
-        weighted = weighted + side[part, 1:2] * new_rows[s : s + 1, :]
-        lat[part, :] = (weighted / side[part, 0:1]).astype(jnp.bfloat16)
-
-    spread = jnp.dot(lat[...], vup[...], preferred_element_type=jnp.float32)
-    own_heads = []
-    head_row = lax.broadcasted_iota(jnp.int32, (seq_count, heads, value_dim), 1)
-    for h in range(heads):
-        block = spread[:, h * value_dim : (h + 1) * value_dim].reshape(seq_count, heads, value_dim)
-        own_heads.append(jnp.sum(jnp.where(head_row == h, block, 0.0), axis=1))
-    hbuf[me_e] = jnp.concatenate(own_heads, axis=1).astype(jnp.bfloat16)
-
-    for copy in row_copies:
-        copy.wait()
-    xbuf[me_e, :, 0:width] = hidden[...]
-    mark_shape = (seq_count, xbuf.shape[2] - width)
-    mark_row = lax.broadcasted_iota(jnp.int32, mark_shape, 0)
-    mark_lane = lax.broadcasted_iota(jnp.int32, mark_shape, 1)
-    marks = jnp.zeros(mark_shape, jnp.float32)
-    for s in range(seq_count):
-        for j in range(route_of.shape[0]):
-            expert = route_of[j, me_t * seq_count + s]
-            marks = jnp.where((mark_row == s) & (mark_lane == expert), 1.0, marks)
-    xbuf[me_e, :, width:] = marks.astype(jnp.bfloat16)
-
-    pending = []
-
-    def remote(which, mask, source, target, to):
+        own_heads = []
+        head_row = lax.broadcasted_iota(jnp.int32, (unit, heads, value_dim), 1)
+        for h in range(heads):
+            piece = spread[:, h * value_dim : (h + 1) * value_dim].reshape(unit, heads, value_dim)
+            own_heads.append(jnp.sum(jnp.where(head_row == h, piece, 0.0), axis=1))
+        hbuf[c, me_e] = jnp.concatenate(own_heads, axis=1).astype(jnp.bfloat16)
+
+    def remote(group, mask, source, target):
         return pltpu.make_async_remote_copy(
             src_ref=source,
             dst_ref=target,
-            send_sem=ag_send.at[which, mask],
-            recv_sem=ag_recv.at[which, to],
+            send_sem=far_send.at[group],
+            recv_sem=far_recv.at[group],
             device_id=device(flip(me_e, mask, bits), me_t),
             device_id_type=pl.DeviceIdType.MESH,
         )
 
-    def share(which, buf):
+    def share(group, slot):
         for mask in far_first:
-            copy = remote(which, mask, buf.at[me_e], buf.at[me_e], me_e)
-            copy.start()
-            pending.append(copy)
-
-    def arrive(which, buf, mask):
-        e = flip(me_e, mask, bits)
-        remote(which, mask, buf.at[e], buf.at[e], e).wait_recv()
+            remote(group, mask, slot, slot).start()
+
+    peers = pl.ds(0, ep_count - 1)
+    drains = []
+
+    def gathered(group, region):
+        whole = remote(group, 1, region, region)
+        drains.append(whole)
+        whole.wait_recv()
+
+    def columns(c):
+        flat_heads = hbuf[c].reshape(chunk_rows, hbuf.shape[3])
+        cbuf[c, me_e] = jnp.concatenate(
+            [
+                jnp.dot(flat_heads, wo[t], preferred_element_type=jnp.float32)
+                for t in range(wo.shape[0])
+            ],
+            axis=1,
+        ).astype(jnp.bfloat16)
+        share(2 + c, cbuf.at[c, me_e])
+
+    def experts(c):
+        mixed = jnp.concatenate([cbuf[c, o] for o in range(ep_count)], axis=1).astype(jnp.float32)
+        stage = xbuf[:, c].reshape(chunk_rows, xbuf.shape[3])
+        after_mix = (stage[:, :width].astype(jnp.float32) + gains[0] * normalize(mixed)).astype(
+            jnp.bfloat16
+        )
+        mix_rows[c] = after_mix.reshape(ep_count, unit, width)
+        ffn_in = (normalize(after_mix.astype(jnp.float32)) * gains[1]).astype(jnp.bfloat16)
+        norm_rows[c] = ffn_in.reshape(ep_count, unit, width)
+        affinity = jax.nn.sigmoid(
+            lax.dot_general(
+                ffn_in, router[...], (((1,), (1,)), ((), ())), preferred_element_type=jnp.float32
+            )
+        )
+        hot = stage[:, width : width + affinity.shape[1]].astype(jnp.float32)
+        chosen = affinity * hot
+        lane = lax.broadcasted_iota(jnp.int32, chosen.shape, 1)
+        whole = jnp.sum(chosen, axis=1, keepdims=True)
+        outcome = jnp.zeros((chunk_rows, width), jnp.float32)
+        for t in range(ed.shape[0]):
+            mine = jnp.sum(jnp.where(lane == me_e * 2 + t, chosen, 0.0), axis=1, keepdims=True)
+            mine = mine / whole * routed_scale
+            expert_out = swiglu(ffn_in, egu[t, 0], egu[t, 1], ed[t])
+            outcome = outcome + expert_out.astype(jnp.float32) * mine
+        terms[c] = outcome.astype(jnp.bfloat16).reshape(ep_count, unit, width)
+        for mask in far_first:
+            remote(4 + c, mask, terms.at[c, flip(me_e, mask, bits)], back.at[c, me_e]).start()
+        back[c, me_e] = terms[c, me_e]
+
+    for copy in cache_copies[:1]:
+        copy.wait()
+    attend(0)
 
     @pl.when(me_t == 1)
     def _():
@@ -524,68 +581,64 @@
     def _():
         pl.semaphore_wait(ready.at[1], 1)
 
-    share(1, hbuf)
-    share(0, xbuf)
+    share(0, hbuf.at[0, me_e])
+    cross = ep_count // 2
+    remote(7, cross, xbuf.at[me_e], xbuf.at[me_e]).start()
+    for mask in range(cross - 1, 0, -1):
+        remote(6, mask, xbuf.at[me_e], xbuf.at[me_e]).start()
+
+    cache_copies[1].wait()
+    wo_copy = fetch(wo_hbm, wo.at[me_t])
+    gain_copies = [fetch(s, t) for s, t in ((gm_hbm, gm), (gf_hbm, gf), (go_hbm, go))]
+    router_copy = fetch(router_hbm, router)
+    sem = next(sems)
+    fetch(eg_hbm, egu.at[me_t, 0], sem)
+    fetch(eu_hbm, egu.at[me_t, 1], sem)
+    expert_copies = [all_of(egu.at[me_t], sem), fetch(ed_hbm, ed.at[me_t])]
+    sem = next(sems)
+    fetch(sg_hbm, sgu.at[0], sem)
+    fetch(su_hbm, sgu.at[1], sem)
+    shared_copies = [all_of(sgu, sem), fetch(sd_hbm, sd)]
+    attend(1)
+    share(1, hbuf.at[1, me_e])
+
     wo_copy.wait()
     pair_copies[0].wait_recv()
-    for mask in reversed(far_first):
-        arrive(1, hbuf, mask)
-
-    flat_heads = hbuf[...].reshape(total_rows, hbuf.shape[2])
-    cbuf[me_e] = jnp.concatenate(
-        [jnp.dot(flat_heads, wo[t], preferred_element_type=jnp.float32) for t in range(2)], axis=1
-    ).astype(jnp.bfloat16)
-    share(2, cbuf)
-    for mask in reversed(far_first):
-        arrive(0, xbuf, mask)
+    gathered(0, hbuf.at[0, peers])
+    other = flip(me_e, cross, bits)
+    crossed = remote(7, cross, xbuf.at[other], xbuf.at[other])
+    crossed.wait_recv()
+    for mask in range(cross - 1, 0, -1):
+        remote(6, mask, xbuf.at[other], xbuf.at[other]).start()
+    columns(0)
+    gathered(1, hbuf.at[1, peers])
+    columns(1)
     for copy in gain_copies + [router_copy] + expert_copies:
         copy.wait()
     for copy in pair_copies[1:]:
         copy.wait_recv()
-    for mask in reversed(far_first):
-        arrive(2, cbuf, mask)
-
     gains = [ref[...].astype(jnp.float32).reshape(1, width) for ref in (gm, gf, go)]
-    mixed = jnp.concatenate([cbuf[o] for o in range(ep_count)], axis=1).astype(jnp.float32)
-    stage = xbuf[...].reshape(total_rows, xbuf.shape[2])
-    after_mix = (stage[:, :width].astype(jnp.float32) + gains[0] * normalize(mixed)).astype(
-        jnp.bfloat16
-    )
-    mix_rows[...] = after_mix.reshape(mix_rows.shape)
-    ffn_in = (normalize(after_mix.astype(jnp.float32)) * gains[1]).astype(jnp.bfloat16)
-    norm_rows[...] = ffn_in.reshape(norm_rows.shape)
-    affinity = jax.nn.sigmoid(
-        lax.dot_general(
-            ffn_in, router[...], (((1,), (1,)), ((), ())), preferred_element_type=jnp.float32
-        )
-    )
-    hot = stage[:, width : width + affinity.shape[1]].astype(jnp.float32)
-    chosen = affinity * hot
-    lane = lax.broadcasted_iota(jnp.int32, chosen.shape, 1)
-    whole = jnp.sum(chosen, axis=1, keepdims=True)
-    outcome = jnp.zeros((total_rows, width), jnp.float32)
-    for t in range(2):
-        mine = jnp.sum(jnp.where(lane == me_e * 2 + t, chosen, 0.0), axis=1, keepdims=True)
-        mine = mine / whole * routed_scale
-        expert_out = swiglu(ffn_in, eg[t], eu[t], ed[t])
-        outcome = outcome + expert_out.astype(jnp.float32) * mine
-    terms[...] = outcome.astype(jnp.bfloat16).reshape(terms.shape)
-    for mask in far_first:
-        copy = remote(3, mask, terms.at[flip(me_e, mask, bits)], back.at[me_e], me_e)
-        copy.start()
-        pending.append(copy)
+    gathered(2, cbuf.at[0, peers])
+    gathered(6, xbuf.at[pl.ds(0, ep_count - 2)])
+    experts(0)
+    gathered(3, cbuf.at[1, peers])
+    experts(1)
     for copy in shared_copies:
         copy.wait()
-    combined = terms[me_e].astype(jnp.float32) + swiglu(
-        norm_rows[me_e], sg[...], su[...], sd[...]
-    ).astype(jnp.float32)
-    for mask in reversed(far_first):
-        arrive(3, back, mask)
-        combined = combined + back[flip(me_e, mask, bits)].astype(jnp.float32)
-    out_ref[...] = (
-        mix_rows[me_e].astype(jnp.float32) + gains[2] * normalize(combined)
+    own_in = jnp.concatenate(
+        [norm_rows[c, me_e].astype(jnp.float32) for c in range(chunks)], axis=0
     ).astype(jnp.bfloat16)
-    for copy in pending + pair_copies:
+    combined = swiglu(own_in, sgu[0], sgu[1], sd[...]).astype(jnp.float32)
+    returned = []
+    for c in range(chunks):
+        gathered(4 + c, back.at[c, peers])
+        returned.append(jnp.sum(back[c].astype(jnp.float32), axis=0))
+    combined = combined + jnp.concatenate(returned, axis=0)
+    own_mix = jnp.concatenate(
+        [mix_rows[c, me_e].astype(jnp.float32) for c in range(chunks)], axis=0
+    )
+    out_ref[...] = (own_mix + gains[2] * normalize(combined)).astype(jnp.bfloat16)
+    for copy in pair_copies + [crossed] + drains:
         copy.wait_send()
 
 
@@ -620,6 +673,8 @@
     bf = jnp.bfloat16
     score_scale = (query_nope.shape[-1] + query_rope.shape[-1]) ** (-0.5)
     dma = pltpu.SemaphoreType.DMA
+    chunks = 2
+    unit = seq_count // chunks
     total_rows = ep_count * seq_count
     rows = seq_count * heads
     depth = seq_count * (latent + rope)
@@ -671,32 +726,29 @@
             near(value_up),
             near(out_proj, (2,)),
             near(router_rows),
-            near(gate, (2,)),
-            near(up, (2,)),
+            near(gate, (2, 2)),
             near(down, (2,)),
-            near(shared_gate),
-            near(shared_up),
+            near(shared_gate, (2,)),
             near(shared_down),
             pltpu.VMEM((latent, heads * value_up.shape[2]), bf),
             pltpu.VMEM((depth, rows), bf),
             pltpu.VMEM((8, depth), jnp.float32),
+            pltpu.VMEM((context, rows), jnp.float32),
+            pltpu.VMEM((rows, context), bf),
             pltpu.VMEM((rows, latent), bf),
-            pltpu.VMEM((ep_count, seq_count, width + 128), bf),
-            pltpu.VMEM((ep_count, seq_count, out_proj.shape[0]), bf),
-            pltpu.VMEM((ep_count, total_rows, 2 * out_proj.shape[1]), bf),
-            pltpu.VMEM((ep_count, seq_count, width), bf),
-            pltpu.VMEM((ep_count, seq_count, width), bf),
-            pltpu.VMEM((ep_count, seq_count, width), bf),
-            pltpu.VMEM((ep_count, seq_count, width), bf),
-            dma((len(operands),)),
-            dma((seq_count,)),
+            pltpu.VMEM((ep_count, chunks, unit, width + 128), bf),
+            pltpu.VMEM((chunks, ep_count, unit, out_proj.shape[0]), bf),
+            pltpu.VMEM((chunks, ep_count, ep_count * unit, 2 * out_proj.shape[1]), bf),
+            pltpu.VMEM((chunks, ep_count, unit, width), bf),
+            pltpu.VMEM((chunks, ep_count, unit, width), bf),
+            pltpu.VMEM((chunks, ep_count, unit, width), bf),
+            pltpu.VMEM((chunks, ep_count, unit, width), bf),
+            dma((21,)),
             dma((4,)),
             dma((4,)),
-            dma((4, ep_count)),
-            dma((4, ep_count)),
+            dma((8,)),
+            dma((8,)),
             pltpu.SemaphoreType.REGULAR((2,)),
-            pltpu.VMEM((context, rows), jnp.float32),
-            pltpu.VMEM((rows, context), bf),
         ],
         compiler_params=pltpu.CompilerParams(
             collective_id=0, has_side_effects=True, vmem_limit_bytes=56 * 2**20

time: 36.8 us -> 29.8 us (0.81)
  Pallas kernels: 36 us -> 29 us
    pallas_call x1, Pallas kernels: 36 us -> 29 us  [local_fused(): pl.pallas_call(functools.partial(fused_kernel, ep_count, score_scale), ou...]
where the time goes in v3:
time: 29.8 us; the launch traced here: 29.6 us
  Pallas kernels  29 us (97%)
  local copies, waits for them, and re-layouts  0.62 us (2%)
    pallas_call x1, Pallas kernels, local_fused(): pl.pallas_call(functools.partial(fused_kernel, ep_count, score_scale), ou...  29 us
    unnamed x1, local copies, waits for them, and re-layouts  0.62 us

profile of v3, /device:TPU:0, one launch (start us, length us, event | category | flops | bytes accessed | tf_op | source)
XLA Modules:
  0.0 29.6 jit_solution(7115587116352774506)
XLA Ops:
  0.0 29.0 %layer_step.1 = bf16[8,2048]{1,0:T(8,128)(2,1)S(1)} custom-call(bf16[8,2048]{1,0:T(8,128)(2,1)} %hidden_hbm.1, bf16[8,16,64]{2,1,0:T(8,128)(2,1)} %qn_hbm.1, bf16[8,16,32]{2,1,0:T(8,128)(2,1)} %qr_hbm.1, bf16[8,256]{1,0:T(8,128)(2,1)} %nl_hbm.1, bf16[8,32]{1,0:T(8,128)(2,1)} %nr_hbm.1, s32[8]{0:T(128)} %len_hbm.1, s32[6,16]{1,0:T(8,128)} %bitcast.17, ...), custom_call_target="tpu_custom_call" | custom-call | flops 33554432 | bytes 16777216 | tf_op jit(solution)/shard_map/layer_step/pallas_call | solution.py:715
  29.0 0.6 %copy.24 = bf16[8,2048]{1,0:T(8,128)(2,1)} copy(bf16[8,2048]{1,0:T(8,128)(2,1)S(1)} %layer_step.1) | data formatting | bytes 65536

commit v4 on v3

--- a/solution.py
+++ b/solution.py
@@ -297,9 +297,9 @@
     query_copies = [
         fetch(s, t) for s, t in ((qr_hbm, qr), (nl_hbm, nl), (nr_hbm, nr), (qn_hbm, qn))
     ]
+    row_copies = [fetch(routes_hbm, route_of), fetch(hidden_hbm, hidden)]
     absorb_copy = fetch(ab_hbm, ab)
     value_copy = fetch(vup_hbm, vraw)
-    row_copies = [fetch(routes_hbm, route_of), fetch(hidden_hbm, hidden)]
     rope_copy = fetch(cr_hbm, rope_keys)
     cache_copies = []
     for c in range(chunks):
@@ -360,7 +360,8 @@
     inverse = jnp.zeros((seq_count, rope), jnp.float32)
     for i in range(half):
         inverse = jnp.where(turn_lane % half == i, rope_theta ** (-2.0 * i / rope), inverse)
-    len_copy.wait()
+    for copy in [len_copy, absorb_copy] + query_copies:
+        copy.wait()
     position = jnp.zeros((seq_count, rope), jnp.float32)
     for s in range(seq_count):
         position = jnp.where(turn_row == s, length_of[s].astype(jnp.float32), position)
@@ -375,8 +376,6 @@
     def per_head(table):
         return jnp.broadcast_to(table[:, None, :], (seq_count, heads, rope)).reshape(rows, rope)
 
-    for copy in query_copies:
-        copy.wait()
     query_rows = qr[...].astype(jnp.float32).reshape(rows, rope)
     q_pe = turned(query_rows, per_head(cosine), per_head(sine))
     key_rows = turned(nr[...].astype(jnp.float32), cosine, sine)
@@ -408,7 +407,6 @@
         ],
         axis=1,
     )
-    absorb_copy.wait()
     q_lat = jnp.dot(spread_query, ab[...], preferred_element_type=jnp.float32)
     q_turned = q_lat.T
     lane_seq = lax.broadcasted_iota(jnp.int32, (latent, rows), 1) // heads
@@ -419,7 +417,8 @@
         wq[place, :] = jnp.where(lane_seq == s, q_turned, 0.0).astype(jnp.bfloat16)
         wq[rope_place, :] = jnp.where(rope_seq == s, rope_turned, 0.0).astype(jnp.bfloat16)
 
-    value_copy.wait()
+    for copy in row_copies + [value_copy, rope_copy]:
+        copy.wait()
     for b in range(0, latent // step, 2):
         blocks = [
             vraw[i * step : (i + 1) * step].reshape(step * heads, value_dim) for i in (b, b + 1)
@@ -433,8 +432,6 @@
                     ordered[h * step : (h + 1) * step, i * value_dim : (i + 1) * value_dim]
                 )
 
-    for copy in row_copies:
-        copy.wait()
     mark_shape = (seq_count, xbuf.shape[3] - width)
     mark_row = lax.broadcasted_iota(jnp.int32, mark_shape, 0)
     mark_lane = lax.broadcasted_iota(jnp.int32, mark_shape, 1)
@@ -457,7 +454,6 @@
     new_score = jnp.dot(
         new_keys[...].astype(jnp.bfloat16), wq[...], preferred_element_type=jnp.float32
     )[0:1]
-    rope_copy.wait()
     for c in range(chunks):
         at = c * chunk_depth + unit * latent
         keys[:, at : at + unit * rope] = rope_keys[c * unit * rope : (c + 1) * unit * rope].T
@@ -568,24 +564,41 @@
             remote(4 + c, mask, terms.at[c, flip(me_e, mask, bits)], back.at[c, me_e]).start()
         back[c, me_e] = terms[c, me_e]
 
-    for copy in cache_copies[:1]:
-        copy.wait()
+    cross = ep_count // 2
+    upper = me_e >= cross
+
+    def open_plane():
+        @pl.when(me_t == 1)
+        def _():
+            pl.semaphore_wait(barrier, ep_count - 1)
+            tell(ready.at[1], sibling)
+
+        @pl.when(me_t == 0)
+        def _():
+            pl.semaphore_wait(ready.at[1], 1)
+
+    def spread_rows():
+        remote(7, cross, xbuf.at[me_e], xbuf.at[me_e]).start()
+        for mask in range(cross - 1, 0, -1):
+            remote(6, mask, xbuf.at[me_e], xbuf.at[me_e]).start()
+
+    @pl.when(upper)
+    def _():
+        open_plane()
+        spread_rows()
+
+    cache_copies[0].wait()
     attend(0)
 
-    @pl.when(me_t == 1)
+    @pl.when(jnp.logical_not(upper))
     def _():
-        pl.semaphore_wait(barrier, ep_count - 1)
-        tell(ready.at[1], sibling)
-
-    @pl.when(me_t == 0)
+        open_plane()
+
+    share(0, hbuf.at[0, me_e])
+
+    @pl.when(jnp.logical_not(upper))
     def _():
-        pl.semaphore_wait(ready.at[1], 1)
-
-    share(0, hbuf.at[0, me_e])
-    cross = ep_count // 2
-    remote(7, cross, xbuf.at[me_e], xbuf.at[me_e]).start()
-    for mask in range(cross - 1, 0, -1):
-        remote(6, mask, xbuf.at[me_e], xbuf.at[me_e]).start()
+        spread_rows()
 
     cache_copies[1].wait()
     wo_copy = fetch(wo_hbm, wo.at[me_t])
@@ -765,6 +778,7 @@
     fits = (
         lax.axis_size("tp") == 2
         and ep_count & (ep_count - 1) == 0
+        and ep_count >= 8
         and hidden_in.shape[0] == 8
         and args[1].shape[1] == 16
         and device_count * hidden_in.shape[0] <= 256

time: 29.8 us -> 29.1 us (0.977)
  Pallas kernels: 29 us -> 28.3 us
    pallas_call x1, Pallas kernels: 29 us -> 28.3 us  [local_fused(): pl.pallas_call(functools.partial(fused_kernel, ep_count, score_scale), ou...]
where the time goes in v4:
time: 29.1 us; the launch traced here: 28.9 us
  Pallas kernels  28.3 us (97%)
  local copies, waits for them, and re-layouts  0.62 us (2%)
    pallas_call x1, Pallas kernels, local_fused(): pl.pallas_call(functools.partial(fused_kernel, ep_count, score_scale), ou...  28.3 us
    unnamed x1, local copies, waits for them, and re-layouts  0.62 us

profile of v4, /device:TPU:0, one launch (start us, length us, event | category | flops | bytes accessed | tf_op | source)
XLA Modules:
  0.0 28.9 jit_solution(16422156563988401921)
XLA Ops:
  0.0 28.3 %layer_step.1 = bf16[8,2048]{1,0:T(8,128)(2,1)S(1)} custom-call(bf16[8,2048]{1,0:T(8,128)(2,1)} %hidden_hbm.1, bf16[8,16,64]{2,1,0:T(8,128)(2,1)} %qn_hbm.1, bf16[8,16,32]{2,1,0:T(8,128)(2,1)} %qr_hbm.1, bf16[8,256]{1,0:T(8,128)(2,1)} %nl_hbm.1, bf16[8,32]{1,0:T(8,128)(2,1)} %nr_hbm.1, s32[8]{0:T(128)} %len_hbm.1, s32[6,16]{1,0:T(8,128)} %bitcast.17, ...), custom_call_target="tpu_custom_call" | custom-call | flops 33554432 | bytes 16777216 | tf_op jit(solution)/shard_map/layer_step/pallas_call | solution.py:728
  28.3 0.6 %copy.24 = bf16[8,2048]{1,0:T(8,128)(2,1)} copy(bf16[8,2048]{1,0:T(8,128)(2,1)S(1)} %layer_step.1) | data formatting | bytes 65536
